TPU v7x, 512 devices: a 8x2x16 block of a 8x16x16 slice. The times are simulated.
512 devices in a mesh: grp: 2 (over y), sp: 16 (over z), tp: 16 (over x, core).
Axes of the slice: x: 8, y: 2, z: 16, core: 2. Of those that a mesh axis runs over, the one named last changes fastest.
The devices are a block of a 8x16x16 slice.
Arguments:
- resid: bfloat16 [8192, 2048], P(('grp', 'sp', 'tp')), parts along dimension 0, may hold values from -6 to 6
- gate_b: bfloat16 [8192, 2048], P(('grp', 'sp'), 'tp'), parts along dimension 0, may hold values from -6 to 6
- gate_c: bfloat16 [8192, 2048], P(('grp', 'sp'), 'tp'), parts along dimension 0, may hold values from -6 to 6
- value: bfloat16 [8192, 2048], P(('grp', 'sp'), 'tp'), parts along dimension 0, may hold values from -6 to 6
- taps: bfloat16 [3, 2048], P(None, 'tp'), may hold values from -3.5 to 3.5
- doc_ids: int32 [8192], P(('grp', 'sp')), parts along dimension 0, may hold values from 0 to 3, never falling along the last dimension, each value on 1 to 2048 neighbouring positions
- out_weight: bfloat16 [2048, 2048], P('tp'), may hold values from -0.125 to 0.125
- norm_gains: float32 [3, 2048], replicated, may hold values from 0.1 to 1.9
- routes: int32 [8192, 2], P(('grp', 'sp')), parts along dimension 0, may hold values from 0 to 15, all different within a row; in each aligned block of 16 rows (0 to 15, 16 to 31, ...) at most 3 rows name the same one
- route_weights: float32 [8192, 2], P(('grp', 'sp')), parts along dimension 0, may hold values from 0.2 to 1
- w_gate: bfloat16 [16, 2048, 4096], P('sp', None, 'tp'), may hold values from -0.125 to 0.125
- w_up: bfloat16 [16, 2048, 4096], P('sp', None, 'tp'), may hold values from -0.125 to 0.125
- w_down: bfloat16 [16, 4096, 2048], P('sp', 'tp'), may hold values from -0.09375 to 0.09375
Outputs:
- layer_out: bfloat16 [8192, 2048], P(('grp', 'sp', 'tp')), parts along dimension 0
There are 2 independent parts, one for each index of `grp`. A program takes and returns all parts, laid end to end along the dimension named above; an argument that names none is the same for every part. Nothing has to cross between parts.
Inputs may be any that keep to these rules, and one draw needn't show every extreme that they name: `doc_ids`: never falling along the sequence; each document spans 1 to 2048 positions. `routes`: each row names 2 different experts. In each aligned block of 16 rows no expert is named more than 3 times, and in every draw some block names some expert exactly 3 times.
All inputs are finite; a program needn't handle non-finite values.
Results may differ from a plain program's by a relative error of at most 0.02.
Values may be sent and summed in bfloat16 or wider, within the bound.
A program may use at most 64 MiB of HBM per device.

v0:
```python
import jax
import jax.numpy as jnp
from jax import lax
from jax.sharding import PartitionSpec as P

TAPS = 3
TOP = 2


norm_eps = 1e-06


def passed_along(block, axis, distance):
    devices = range(lax.axis_size(axis))
    route = [(i - distance, i) for i in devices if i - distance in devices]
    return lax.ppermute(block, axis, route)


def in_blocks(array, dim, length):
    before, after = (array.shape[:dim], array.shape[dim + 1 :])
    return jnp.moveaxis(array.reshape(*before, length, -1, *after), dim, 0)


def sent_and_summed(array, axis, dim):
    tiles = in_blocks(array, dim, lax.axis_size(axis))
    arrived = lax.all_to_all(tiles, axis, split_axis=0, concat_axis=0, tiled=True)
    return arrived.astype(jnp.float32).sum(axis=0)


def rms_scale(values, gain_row):
    mean_sq = jnp.mean(values * values, axis=-1, keepdims=True)
    return values * lax.rsqrt(mean_sq + norm_eps) * gain_row


def slot_table(block_routes, experts, capacity):
    block_count = block_routes.shape[0]
    block_len = block_routes.shape[1]
    flat_routes = block_routes.reshape(block_count, block_len * TOP)
    onehot = (
        flat_routes[:, :, None] == jnp.arange(experts, dtype=jnp.int32)[None, None, :]
    ).astype(jnp.int32)
    before = jnp.cumsum(onehot, axis=1) - onehot
    slot_rank = jnp.sum(before * onehot, axis=2)
    slot_hit = onehot[:, :, :, None] * (
        slot_rank[:, :, None, None] == jnp.arange(capacity, dtype=jnp.int32)[None, None, None, :]
    ).astype(jnp.int32)
    owner_row = jnp.arange(block_len * TOP, dtype=jnp.int32) // TOP
    slot_tok = jnp.sum(slot_hit * owner_row[None, :, None, None], axis=1)
    filled = jnp.sum(slot_hit, axis=1)
    return (slot_rank.reshape(block_count, block_len, TOP), slot_tok, filled)


def pick_rows(normed_rows, slot_tok, filled):
    picked_rows = normed_rows[slot_tok]
    return jnp.where(filled[:, :, None] > 0, picked_rows, jnp.zeros_like(picked_rows))


def expert_hidden(picked_rows, w_gate, w_up):
    gate_proj = jnp.dot(picked_rows, w_gate[0], preferred_element_type=jnp.float32)
    up_proj = jnp.dot(picked_rows, w_up[0], preferred_element_type=jnp.float32)
    return (jax.nn.silu(gate_proj) * up_proj).astype(jnp.bfloat16)


def per_device(
    resid,
    gate_b,
    gate_c,
    value,
    taps,
    doc_ids,
    out_weight,
    norm_gains,
    routes,
    route_weights,
    w_gate,
    w_up,
    w_down,
):
    tok_dev = gate_b.shape[0]
    rows_blk = resid.shape[0]
    model_width = resid.shape[1]
    experts = lax.axis_size("sp")
    capacity = max(2, 3 * TOP * rows_blk // (2 * experts))
    tap_reach = TAPS - 1
    product = gate_c.astype(jnp.float32) * value.astype(jnp.float32)
    id_values = doc_ids.astype(jnp.float32)
    prev_rows, prev_ids = passed_along(
        (product[tok_dev - tap_reach :], id_values[tok_dev - tap_reach :]), "sp", 1
    )
    ext_rows = jnp.concatenate([prev_rows, product], axis=0)
    ext_ids = jnp.concatenate([prev_ids, id_values], axis=0)
    tap_weights = taps.astype(jnp.float32)
    convolved = tap_weights[0] * product
    for distance in range(1, TAPS):
        earlier = ext_rows[tap_reach - distance : tap_reach - distance + tok_dev]
        same_doc = ext_ids[tap_reach - distance : tap_reach - distance + tok_dev] == id_values
        convolved = convolved + jnp.where(same_doc[:, None], tap_weights[distance] * earlier, 0.0)
    mixed_rows = (gate_b.astype(jnp.float32) * convolved).astype(jnp.bfloat16)
    block_rows = mixed_rows
    projected = sent_and_summed(
        jnp.dot(block_rows, out_weight, preferred_element_type=jnp.float32).astype(jnp.bfloat16),
        "tp",
        0,
    )
    stream = resid.astype(jnp.float32) + rms_scale(projected, norm_gains[0])
    normed = rms_scale(stream, norm_gains[1]).astype(jnp.bfloat16)
    lane_index = lax.axis_index("tp")
    offset = lane_index * rows_blk
    my_routes = lax.dynamic_slice_in_dim(routes, offset, rows_blk, 0)
    my_weights = lax.dynamic_slice_in_dim(route_weights, offset, rows_blk, 0)
    own_rank, own_tok, own_filled = slot_table(my_routes[None], experts, capacity)
    slot_rank = own_rank[0]
    outgoing = pick_rows(normed, own_tok[0], own_filled[0])
    arrived = lax.all_to_all(outgoing, "sp", split_axis=0, concat_axis=0, tiled=True)
    hidden = expert_hidden(
        lax.all_gather(arrived[None], "tp", axis=0, tiled=True).reshape(-1, model_width),
        w_gate,
        w_up,
    )
    block_rows = hidden
    summed = lax.psum_scatter(
        jnp.dot(block_rows, w_down[0], preferred_element_type=jnp.float32).astype(jnp.bfloat16),
        "tp",
        scatter_dimension=0,
        tiled=True,
    )
    results = summed.reshape(experts, capacity, model_width)
    returned = lax.all_to_all(results, "sp", split_axis=0, concat_axis=0, tiled=True)
    picked = returned[my_routes, slot_rank]
    shares = my_weights / jnp.sum(my_weights, axis=1, keepdims=True)
    combined = jnp.sum(shares[:, :, None] * picked.astype(jnp.float32), axis=1)
    return (stream + rms_scale(combined, norm_gains[2])).astype(jnp.bfloat16)


def solution(mesh):
    return jax.shard_map(
        per_device,
        mesh=mesh,
        in_specs=(
            P(("grp", "sp", "tp"), None),
            P(("grp", "sp"), "tp"),
            P(("grp", "sp"), "tp"),
            P(("grp", "sp"), "tp"),
            P(None, "tp"),
            P(("grp", "sp")),
            P("tp", None),
            P(),
            P(("grp", "sp"), None),
            P(("grp", "sp"), None),
            P("sp", None, "tp"),
            P("sp", None, "tp"),
            P("sp", "tp", None),
        ),
        out_specs=P(("grp", "sp", "tp"), None),
        check_vma=False,
    )
```

profile of v0, /device:TPU:80, one launch (start us, length us, event | category | flops | bytes accessed | tf_op | source)
XLA Modules:
  0.0 291.9 jit_solution(14449329328354354101)
XLA Ops:
  6.5 0.0 copy-start
  6.6 0.8 convert_element_type.76
  7.3 0.1 slice.37
  7.4 6.0 %collective-permute-start = (f32[2]{0:T(128)S(1)}, f32[2]{0:T(128)S(1)}, u32[]{:S(2)}, u32[]{:S(2)}) collective-permute-start(f32[2]{0:T(128)S(1)} %slice.37), channel_id=1, source_target_pairs={{0,16},{16,32},{32,48},{48,64},{64,80},{80,96},{96,112},{112,128},... | collective-permute-start | bytes 32 | tf_op jit(solution)/shard_map/ppermute | solution.py:16
  13.4 0.9 convert_multiply_fusion
  14.3 6.0 %collective-permute-start.1 = (f32[2,128]{1,0:T(2,128)S(1)}, f32[2,128]{1,0:T(2,128)S(1)}, u32[]{:S(2)}, u32[]{:S(2)}) collective-permute-start(f32[2,128]{1,0:T(2,128)S(1)} %slice.52), channel_id=1, source_target_pairs={{0,16},{16,32},{32,48},{48,64},{64,80},{80,96},{96,112},{112,128},... | collective-permute-start | bytes 3080 | tf_op jit(solution)/shard_map/ppermute | solution.py:16
  20.4 0.7 convert_element_type.73
  21.1 0.7 constant_dynamic-slice_fusion
  21.8 0.1 copy.41
  21.9 0.1 eq.63
  22.0 0.0 collective-permute-done
  22.0 0.1 pad_maximum_fusion.1
  22.1 0.8 slice_compare_fusion.1
  22.8 0.0 collective-permute-done.1
  22.8 2.6 convolution_convert_fusion.1
  25.4 7.6 %all-to-all-start = ((bf16[16,16,2048]{2,1,0:T(8,128)(2,1)}), bf16[16,16,2048]{2,1,0:T(8,128)(2,1)S(1)}, u32[]{:S(2)}, u32[]{:S(2)}) async-start(bf16[16,16,2048]{2,1,0:T(8,128)(2,1)} %bitcast.3), calls=%async_computation | async-start | bytes 2097152 | tf_op jit(solution)/shard_map/all_to_all | solution.py:26
  33.0 0.1 all-gather.3.cloned.1.call-start
  33.1 0.1 fusion.29
  33.2 0.1 reduce_window_sum.11
  33.2 0.2 select_reduce_fusion
  33.4 0.2 multiply_reduce_fusion.4
  33.6 0.1 copy.43
  33.7 0.1 reshape.258
  33.8 0.1 copy.42
  33.9 0.0 copy-done.2
  34.0 25.4 %all-to-all-done = bf16[16,16,2048]{2,1,0:T(8,128)(2,1)S(1)} async-done(((bf16[16,16,2048]{2,1,0:T(8,128)(2,1)}), bf16[16,16,2048]{2,1,0:T(8,128)(2,1)S(1)}, u32[]{:S(2)}, u32[]{:S(2)}) %all-to-all-start) | async-done | bytes 1048608 | tf_op jit(solution)/shard_map/all_to_all | solution.py:26
  59.3 0.1 convert_reduce_fusion
  59.5 0.1 multiply_reduce_fusion.3
  59.6 0.0 copy-done.1
  59.6 0.2 multiply_reduce_fusion.2
  59.8 0.1 multiply_convert_fusion
  59.9 0.7 gather_fusion
  60.6 0.1 reshape.257
  60.8 0.2 broadcast_select_fusion
  61.0 53.7 %all_to_all.15 = bf16[16,3,2048]{2,1,0:T(4,128)(2,1)S(1)} all-to-all(bf16[16,3,2048]{2,1,0:T(4,128)(2,1)S(1)} %broadcast_select_fusion), channel_id=1, replica_groups=mesh['grp'=2,'sp'=16,'tp'=16] {'sp'}, dimensions={0} | all-to-all | bytes 393216 | tf_op jit(solution)/shard_map/all_to_all | solution.py:114
  114.6 0.8 copy.44
  115.4 0.1 all-gather.3.cloned.1.call-update
  115.5 0.1 reduce-scatter.2.cloned.1.call-start
  115.6 42.3 %all-gather.3.cloned.1.call-done = bf16[256,3,2048]{2,0,1:T(8,128)(2,1)} async-done(((bf16[16,3,2048]{2,0,1:T(8,128)(2,1)}), bf16[256,3,2048]{2,0,1:T(8,128)(2,1)}) %all-gather.3.cloned.1.call-update) | async-done | bytes 3145744 | tf_op jit(solution)/shard_map/all_gather | solution.py:116
  157.9 6.5 %copy.45 = bf16[256,3,2048]{2,1,0:T(4,128)(2,1)} copy(bf16[256,3,2048]{2,0,1:T(8,128)(2,1)} %all-gather.3.cloned.1.call-done) | data formatting | bytes 6291456 | tf_op jit(solution)/shard_map/all_gather | solution.py:116
  164.4 8.9 %reshape.254 = bf16[768,2048]{1,0:T(8,128)(2,1)} reshape(bf16[256,3,2048]{2,1,0:T(4,128)(2,1)} %copy.45) | data formatting | bytes 6291456 | tf_op jit(solution)/shard_map/reshape | solution.py:116
  173.3 0.0 copy-done.5
  173.3 3.8 %fusion.4 = f32[768,256]{1,0:T(8,128)} fusion(bf16[768,2048]{1,0:T(8,128)(2,1)} %reshape.254, bf16[1,2048,256]{2,1,0:T(8,128)(2,1)S(1)} %copy-done.5), kind=kOutput, calls=%fused_computation.9 | convolution fusion | flops 805306368 | bytes 4980736 | tf_op jit(solution)/shard_map/dot_general | solution.py:59
  177.2 0.0 copy-done.6
  177.2 7.1 %convolution_convert_fusion = bf16[768,2048]{1,0:T(8,128)(2,1)} fusion(bf16[768,2048]{1,0:T(8,128)(2,1)} %reshape.254, bf16[1,256,2048]{2,1,0:T(8,128)(2,1)S(1)} %copy-done, bf16[1,2048,256]{2,1,0:T(8,128)(2,1)S(1)} %copy-done.6, f32[768,256]{1,0:T(8,128)} %fusion.4), kind=kOutput, calls=%fused_computation.2 | convolution fusion | flops 1613365248 | bytes 9175040 | tf_op jit(solution)/shard_map/dot_general | solution.py:122
  184.3 0.1 reduce-scatter.2.cloned.1.call-update
  184.3 66.9 %reduce-scatter.2.cloned.1.call-done = bf16[48,2048]{1,0:T(8,128)(2,1)} async-done(((bf16[768,2048]{1,0:T(8,128)(2,1)}), bf16[48,2048]{1,0:T(8,128)(2,1)}) %reduce-scatter.2.cloned.1.call-update) | async-done | bytes 196624 | tf_op jit(solution)/shard_map/reduce_scatter | solution.py:121
  251.2 1.7 reshape.255
  252.9 13.1 %all-to-all-start.2 = ((bf16[16,3,2048]{2,1,0:T(4,128)(2,1)}), bf16[16,3,2048]{2,1,0:T(4,128)(2,1)S(1)}, u32[]{:S(2)}, u32[]{:S(2)}) async-start(bf16[16,3,2048]{2,1,0:T(4,128)(2,1)} %reshape.255), calls=%async_computation.3 | async-start | bytes 524288 | tf_op jit(solution)/shard_map/all_to_all | solution.py:128
  266.1 0.1 squeeze_reshape.3
  266.1 0.1 copy.46
  266.2 0.1 fusion.35
  266.3 0.1 copy.49
  266.4 0.1 reshape.264
  266.5 0.1 dynamic-slice_reduce_fusion
  266.6 0.1 dynamic-slice_divide_fusion
  266.7 0.1 copy.40
  266.8 15.7 %all-to-all-done.2 = bf16[16,3,2048]{2,1,0:T(4,128)(2,1)S(1)} async-done(((bf16[16,3,2048]{2,1,0:T(4,128)(2,1)}), bf16[16,3,2048]{2,1,0:T(4,128)(2,1)S(1)}, u32[]{:S(2)}, u32[]{:S(2)}) %all-to-all-start.2) | async-done | bytes 196640 | tf_op jit(solution)/shard_map/all_to_all | solution.py:128
  282.4 0.1 copy.50
  282.6 1.0 gather_fusion.1
  283.6 0.2 reshape.273
  283.8 0.4 multiply_reduce_fusion
  284.2 0.1 multiply_reduce_fusion.1
  284.3 0.7 add_convert_fusion
  (21 shorter events, 0.1 us)
Async XLA Ops:
  6.5 170.6 %copy-start = (bf16[1,256,2048]{2,1,0:T(8,128)(2,1)S(1)}, bf16[1,256,2048]{2,1,0:T(8,128)(2,1)}, u32[]{:S(2)}) copy-start(bf16[1,256,2048]{2,1,0:T(8,128)(2,1)} %param.25) | copy-start | bytes 3145732
  6.6 27.4 %copy-start.2 = (f32[3,2048]{1,0:T(4,128)S(1)}, f32[3,2048]{1,0:T(4,128)}, u32[]{:S(2)}) copy-start(f32[3,2048]{1,0:T(4,128)} %param.20) | copy-start | bytes 73732
  6.6 53.0 %copy-start.1 = (bf16[16,2048]{1,0:T(8,128)(2,1)S(1)}, bf16[16,2048]{1,0:T(8,128)(2,1)}, u32[]{:S(2)}) copy-start(bf16[16,2048]{1,0:T(8,128)(2,1)} %param.13) | copy-start | bytes 196612
  7.4 14.6 %collective-permute-start = (f32[2]{0:T(128)S(1)}, f32[2]{0:T(128)S(1)}, u32[]{:S(2)}, u32[]{:S(2)}) collective-permute-start(f32[2]{0:T(128)S(1)} %slice.37), channel_id=1, source_target_pairs={{0,16},{16,32},{32,48},{48,64},{64,80},{80,96},{96,112},{112,128},... | collective-permute-start | bytes 32 | tf_op jit(solution)/shard_map/ppermute | solution.py:16
  14.3 8.5 %collective-permute-start.1 = (f32[2,128]{1,0:T(2,128)S(1)}, f32[2,128]{1,0:T(2,128)S(1)}, u32[]{:S(2)}, u32[]{:S(2)}) collective-permute-start(f32[2,128]{1,0:T(2,128)S(1)} %slice.52), channel_id=1, source_target_pairs={{0,16},{16,32},{32,48},{48,64},{64,80},{80,96},{96,112},{112,128},... | collective-permute-start | bytes 3080 | tf_op jit(solution)/shard_map/ppermute | solution.py:16
  25.4 33.9 %all-to-all-start = ((bf16[16,16,2048]{2,1,0:T(8,128)(2,1)}), bf16[16,16,2048]{2,1,0:T(8,128)(2,1)S(1)}, u32[]{:S(2)}, u32[]{:S(2)}) async-start(bf16[16,16,2048]{2,1,0:T(8,128)(2,1)} %bitcast.3), calls=%async_computation | async-start | bytes 2097152 | tf_op jit(solution)/shard_map/all_to_all | solution.py:26
  33.0 124.9 %all-gather.3.cloned.1.call-start = ((), (), s32[]{:S(2)}) async-start(), calls=%async_computation.5 | async-start | bytes 3342336 | tf_op jit(solution)/shard_map/all_gather | solution.py:116
  115.5 135.7 %reduce-scatter.2.cloned.1.call-start = ((), (), s32[]{:S(2)}) async-start(), calls=%async_computation.4 | async-start | bytes 3342336 | tf_op jit(solution)/shard_map/reduce_scatter | solution.py:121
  164.4 8.9 %copy-start.5 = (bf16[1,2048,256]{2,1,0:T(8,128)(2,1)S(1)}, bf16[1,2048,256]{2,1,0:T(8,128)(2,1)}, u32[]{:S(2)}) copy-start(bf16[1,2048,256]{2,1,0:T(8,128)(2,1)} %param.23) | copy-start | bytes 3145732
  173.3 3.8 %copy-start.6 = (bf16[1,2048,256]{2,1,0:T(8,128)(2,1)S(1)}, bf16[1,2048,256]{2,1,0:T(8,128)(2,1)}, u32[]{:S(2)}) copy-start(bf16[1,2048,256]{2,1,0:T(8,128)(2,1)} %param.24) | copy-start | bytes 3145732
  184.3 82.0 %copy-start.3 = (s32[256,2]{0,1:T(2,128)S(1)}, s32[256,2]{0,1:T(2,128)}, u32[]{:S(2)}) copy-start(s32[256,2]{0,1:T(2,128)} %param.21) | copy-start | bytes 6148
  184.3 82.2 %copy-start.4 = (f32[256,2]{0,1:T(2,128)S(1)}, f32[256,2]{0,1:T(2,128)}, u32[]{:S(2)}) copy-start(f32[256,2]{0,1:T(2,128)} %param.22) | copy-start | bytes 6148
  252.9 29.5 %all-to-all-start.2 = ((bf16[16,3,2048]{2,1,0:T(4,128)(2,1)}), bf16[16,3,2048]{2,1,0:T(4,128)(2,1)S(1)}, u32[]{:S(2)}, u32[]{:S(2)}) async-start(bf16[16,3,2048]{2,1,0:T(4,128)(2,1)} %reshape.255), calls=%async_computation.3 | async-start | bytes 524288 | tf_op jit(solution)/shard_map/all_to_all | solution.py:128
Sparse Core Ops, SparseCore 0:
  115.6 42.2 all-gather.2
  184.5 66.6 reduce-scatter.1
where the time goes:
time: 294 us; the launch traced here: 292 us
  waiting for transfers between devices  150 us (51%)
  blocking collectives  53.7 us (18%)
  starting transfers between devices  32.9 us (11%)
  local copies, waits for them, and re-layouts  21.9 us (7%)
  between operations  13.6 us (5%)
  matrix products  13.5 us (5%)
  other arithmetic  6.01 us (2%)
    reduce_scatter x1, waiting for transfers between devices, per_device(): lax.psum_scatter(jnp.dot(block_rows, w_down[0], preferred_element_type=jn...  66.9 us
    all_to_all x1, blocking collectives, per_device(): lax.all_to_all(outgoing, 'sp', split_axis=0, concat_axis=0, tiled=True)  53.7 us
    all_gather x1, waiting for transfers between devices, per_device(): lax.all_gather(arrived[None], 'tp', axis=0, tiled=True)  42.3 us
    all_to_all x1, waiting for transfers between devices, sent_and_summed(): lax.all_to_all(tiles, axis, split_axis=0, concat_axis=0, tiled=True)  25.4 us
    all_to_all x1, waiting for transfers between devices, per_device(): lax.all_to_all(results, 'sp', split_axis=0, concat_axis=0, tiled=True)  15.7 us
    all_to_all x1, starting transfers between devices, per_device(): lax.all_to_all(results, 'sp', split_axis=0, concat_axis=0, tiled=True)  13.1 us
    ppermute x2, starting transfers between devices, passed_along(): return lax.ppermute(block, axis, route)  12 us
    reshape x1, local copies, waits for them, and re-layouts, per_device(): lax.all_gather(arrived[None], 'tp', axis=0, tiled=True)  8.9 us
  transfers between devices with their start and end apart: 6, of which 4 were waited for; matrix products, arithmetic and copies ran while one was open for 2% of the time, Pallas kernels for 0%

commit v1 on v0

v1 whole, which is shorter than its diff:
```python
import functools

import jax
import jax.numpy as jnp
from jax import lax
from jax.experimental import pallas as pl
from jax.experimental.pallas import tpu as pltpu
from jax.sharding import PartitionSpec as P

TAPS = 3
TOP = 2
LANES = 128
TILE = 16

norm_eps = 1e-06
BF16 = jnp.bfloat16
F32 = jnp.float32
MESH = pl.DeviceIdType.MESH


def rms_scale(values, gain_row):
    mean_sq = jnp.mean(values * values, axis=-1, keepdims=True)
    return values * lax.rsqrt(mean_sq + norm_eps) * gain_row


def layer_kernel(
    n_sp,
    n_tp,
    cap,
    resid,
    gate_b,
    gate_c,
    value,
    taps,
    ids,
    out_w,
    gains,
    routes,
    route_w,
    w_gate,
    w_up,
    w_down,
    out,
    ow,
    wg,
    wu,
    wd,
    ext,
    ext_ids,
    halo_s,
    halo_r,
    mixed,
    sel,
    zs,
    zr,
    bs,
    br,
    fold,
    xbuf,
    hid,
    pair_s,
    pair_r,
    keep,
    ring_s,
    ring_r,
    ring_l,
    stream_ref,
    back,
    w_sem,
    halo_sem,
    z_send,
    z_recv,
    pair_send,
    pair_recv,
    rr_send,
    rr_recv,
    rl_send,
    rl_recv,
    d_send,
    d_recv,
    ar_send,
    ar_recv,
    al_send,
    al_recv,
):
    tok, ch = gate_b.shape
    rows, width = resid.shape
    chips = n_tp // 2
    hops = chips // 2
    half_w = width // 2
    folds = width // LANES
    slots = n_sp * cap
    chunks = slots // TILE
    chunk_rows = n_tp * TILE
    own_rows = chips * TILE
    piece = cap * folds

    tp = lax.axis_index("tp")
    sp = lax.axis_index("sp")
    core = lax.rem(tp, 2)
    chip = lax.div(tp, 2)
    partner = {"tp": chip * 2 + (1 - core)}
    right = {"tp": lax.rem(chip + 1, chips) * 2 + core}
    left = {"tp": lax.rem(chip + chips - 1, chips) * 2 + core}

    def along(d):
        return {"sp": lax.rem(sp + d + n_sp, n_sp)}

    offs = [0] + [
        (p + 1) // 2 if p % 2 else -(p // 2) for p in range(1, n_sp)
    ]

    def pos_of(d):
        return next(p for p in range(n_sp) if (offs[p] - d) % n_sp == 0)

    pending = []

    def send(src, dst, s_sem, r_sem, dev):
        copy = pltpu.make_async_remote_copy(
            src_ref=src,
            dst_ref=dst,
            send_sem=s_sem,
            recv_sem=r_sem,
            device_id=dev,
            device_id_type=MESH,
        )
        copy.start()
        pending.append(copy)
        return copy

    barrier = pltpu.get_barrier_semaphore()
    greeted = [partner, right, left] + [along(d) for d in offs[1:]]
    for dev in greeted:
        pl.semaphore_signal(barrier, inc=1, device_id=dev, device_id_type=MESH)

    loads = [
        pltpu.make_async_copy(out_w, ow, w_sem.at[0]),
        pltpu.make_async_copy(w_gate.at[0], wg, w_sem.at[1]),
        pltpu.make_async_copy(w_up.at[0], wu, w_sem.at[2]),
        pltpu.make_async_copy(w_down.at[0], wd, w_sem.at[3]),
    ]
    for load in loads:
        load.start()

    product = gate_c[...].astype(F32) * value[...].astype(F32)
    ext[pl.ds(8, tok), :] = product
    ext_ids[pl.ds(8, tok), :] = ids[...]
    halo_s[pl.ds(0, 8), :] = product[tok - 8 :]
    halo_s[pl.ds(8, 8), :] = ids[pl.ds(tok - 8, 8), :]

    pl.semaphore_wait(barrier, len(greeted))
    halo = send(halo_s, halo_r, halo_sem.at[0], halo_sem.at[1], along(1))
    halo.wait_recv()
    ext[pl.ds(0, 8), :] = halo_r[pl.ds(0, 8), :]
    ext_ids[pl.ds(0, 8), :] = jnp.where(sp == 0, -1.0, halo_r[pl.ds(8, 8), :])

    here = ext_ids[pl.ds(8, tok), :]
    tap_rows = taps[...].astype(F32)
    conv = tap_rows[0:1, :] * ext[pl.ds(8, tok), :]
    for lag in range(1, TAPS):
        same = ext_ids[pl.ds(8 - lag, tok), :] == here
        conv = conv + jnp.where(
            same, tap_rows[lag : lag + 1, :] * ext[pl.ds(8 - lag, tok), :], 0.0
        )
    mixed[...] = (gate_b[...].astype(F32) * conv).astype(BF16)

    def place(owner, o):
        block = lax.rem(chip + o, chips) * 2 + owner
        return pl.ds(pl.multiple_of(block * rows, rows), rows)

    for o in range(chips):
        sel[0, pl.ds(o * rows, rows), :] = mixed[place(core, o), :]
        sel[1, pl.ds(o * rows, rows), :] = mixed[place(1 - core, o), :]

    ring = {}

    def pair_start(s):
        ring[s, "pair"] = send(
            pair_s.at[s], pair_r.at[s], pair_send.at[s], pair_recv.at[s], partner
        )

    def share(s, o):
        at = pl.ds(o * TILE, TILE)
        return keep[s, at, :] + pair_r[s, at, :].astype(F32)

    def hop_right(s, h, src, dst):
        ring[s, "r", h] = send(
            src, dst, rr_send.at[s, h - 1], rr_recv.at[s, h - 1], right
        )

    def hop_left(s, h, src, dst):
        ring[s, "l", h] = send(
            src, dst, rl_send.at[s, h - 1], rl_recv.at[s, h - 1], left
        )

    lo, hi = pl.ds(0, half_w), pl.ds(half_w, half_w)

    def ring_step(s, h):
        if h == 1:
            ring[s, "pair"].wait_recv()
            ring_s[s, hops] = share(s, hops).astype(BF16)
            hop_right(s, 1, ring_s.at[s, hops, :, lo], ring_r.at[s, 0, :, lo])
            hop_left(s, 1, ring_s.at[s, hops, :, hi], ring_l.at[s, 0, :, hi])
            return
        o = hops + 1 - h
        ring[s, "r", h - 1].wait_recv()
        total = share(s, o)
        if h == 2:
            ring_s[s, o, :, lo] = (
                total[:, :half_w] + ring_r[s, 0, :, lo].astype(F32)
            ).astype(BF16)
            ring_s[s, o, :, hi] = total[:, half_w:].astype(BF16)
        else:
            ring_s[s, o] = (total + ring_r[s, h - 2].astype(F32)).astype(BF16)
        hop_right(s, h, ring_s.at[s, o], ring_r.at[s, h - 1])
        o = chips - o
        ring[s, "l", h - 1].wait_recv()
        total = share(s, o)
        if h == 2:
            ring_s[s, o, :, lo] = total[:, :half_w].astype(BF16)
            ring_s[s, o, :, hi] = (
                total[:, half_w:] + ring_l[s, 0, :, hi].astype(F32)
            ).astype(BF16)
        else:
            ring_s[s, o] = (total + ring_l[s, h - 2].astype(F32)).astype(BF16)
        hop_left(s, h, ring_s.at[s, o], ring_l.at[s, h - 1])

    def ring_end(s):
        ring[s, "r", hops].wait_recv()
        ring[s, "l", hops].wait_recv()
        return (
            share(s, 0)
            + ring_r[s, hops - 1].astype(F32)
            + ring_l[s, hops - 1].astype(F32)
        )

    loads[0].wait()
    step_w = min(512, width)
    for n in range(width // step_w):
        at = pl.ds(n * step_w, step_w)
        pair_s[0, :, at] = jnp.dot(
            sel[1], ow[:, at], preferred_element_type=F32
        ).astype(BF16)
    pair_start(0)
    for n in range(width // step_w):
        at = pl.ds(n * step_w, step_w)
        keep[0, :, at] = jnp.dot(sel[0], ow[:, at], preferred_element_type=F32)
    for h in range(1, hops + 1):
        ring_step(0, h)

    mine = pl.ds(pl.multiple_of(tp * rows, rows), rows)
    my_routes = routes[mine, :]
    my_w = route_w[mine, :]
    lane = lax.broadcasted_iota(jnp.int32, (rows, LANES), 1)
    pos = jnp.floor((lane.astype(F32) + 0.5) * (1.0 / cap)).astype(jnp.int32)
    depth = (lane - pos * cap).astype(F32)
    reach = (pos + 1) >> 1
    away = sp + jnp.where((pos & 1) == 1, reach, -reach)
    away = jnp.where(away < 0, away + n_sp, away)
    away = jnp.where(away >= n_sp, away - n_sp, away)
    expert = jnp.where(lane < slots, away, -1)
    first = (my_routes[:, 0:1] == expert).astype(F32)
    second = (my_routes[:, 1:2] == expert).astype(F32)
    named = first + second
    r_at = lax.broadcasted_iota(jnp.int32, (rows, rows), 0)
    c_at = lax.broadcasted_iota(jnp.int32, (rows, rows), 1)
    earlier = (c_at < r_at).astype(F32).astype(BF16)
    rank = jnp.dot(earlier, named.astype(BF16), preferred_element_type=F32)
    hit = named * (rank == depth).astype(F32)
    total_w = jnp.sum(my_w, axis=1, keepdims=True)
    shares = my_w / total_w
    mix_w = hit * (first * shares[:, 0:1] + second * shares[:, 1:2])
    pick = hit.T.astype(BF16)[:slots, :]

    gain_rows = gains[...]
    projected = ring_end(0)
    stream = resid[...].astype(F32) + rms_scale(projected, gain_rows[0:1, :])
    stream_ref[...] = stream
    normed = rms_scale(stream, gain_rows[1:2, :]).astype(BF16)

    outgoing = jnp.dot(pick, normed, preferred_element_type=F32)
    for b in range(folds):
        fold[pl.ds(b, slots, stride=folds), :] = outgoing[
            :, b * LANES : (b + 1) * LANES
        ]
    folded = fold[...].astype(BF16)
    zs[...] = folded
    zr[pl.ds(0, piece), :] = folded[:piece]

    across = {}

    def z_start(way, src, dst, p):
        q = pos_of(-offs[p])
        across[way, q] = send(
            src.at[pl.ds(p * piece, piece), :],
            dst.at[pl.ds(q * piece, piece), :],
            z_send.at[way, q],
            z_recv.at[way, q],
            along(offs[p]),
        )

    for p in range(1, n_sp):
        z_start(0, zs, zr, p)

    gather = {}
    here_z = [1]

    def block(cc, other, o):
        return pl.ds(cc * chunk_rows + other * own_rows + (o % chips) * TILE, TILE)

    def to_partner(cc, o):
        gather[cc, "d", o % chips] = send(
            xbuf.at[block(cc, 0, o), :],
            xbuf.at[block(cc, 1, o), :],
            d_send.at[cc, o % chips],
            d_recv.at[cc, o % chips],
            partner,
        )

    def hop_out(cc, h):
        if h == 1:
            last = (cc + 1) * TILE * folds
            while here_z[0] < n_sp and here_z[0] * piece < last:
                across[0, here_z[0]].wait_recv()
                here_z[0] += 1
            span = TILE * folds
            fold[pl.ds(0, span), :] = zr[pl.ds(cc * span, span), :].astype(F32)
            for b in range(folds):
                xbuf[block(cc, 0, 0), pl.ds(b * LANES, LANES)] = fold[
                    pl.ds(b, TILE, stride=folds), :
                ].astype(BF16)
        else:
            gather[cc, "r", h - 1].wait_recv()
            gather[cc, "l", h - 1].wait_recv()
        for name, sign, dev, s_sem, r_sem, part in (
            ("r", -1, right, ar_send, ar_recv, lo),
            ("l", 1, left, al_send, al_recv, hi),
        ):
            src = block(cc, 0, sign * (h - 1))
            dst = block(cc, 0, sign * h)
            cols = part if h == hops else slice(None)
            gather[cc, name, h] = send(
                xbuf.at[src, cols],
                xbuf.at[dst, cols],
                s_sem.at[cc, h - 1],
                r_sem.at[cc, h - 1],
                dev,
            )
        to_partner(cc, 1 - h)
        if h > 1:
            to_partner(cc, h - 1)

    def hop_last(cc):
        gather[cc, "r", hops].wait_recv()
        gather[cc, "l", hops].wait_recv()
        to_partner(cc, hops)

    def experts(cc):
        for o in range(chips):
            gather[cc, "d", o].wait_recv()
        s = cc + 1
        x = xbuf[pl.ds(cc * chunk_rows, chunk_rows), :]
        g = jnp.dot(x, wg[...], preferred_element_type=F32)
        u = jnp.dot(x, wu[...], preferred_element_type=F32)
        hid[...] = (g / (1.0 + jnp.exp(-g)) * u).astype(BF16)
        for n in range(width // step_w):
            at = pl.ds(n * step_w, step_w)
            pair_s[s, :, at] = jnp.dot(
                hid[pl.ds(own_rows, own_rows), :],
                wd[:, at],
                preferred_element_type=F32,
            ).astype(BF16)
        pair_start(s)
        for n in range(width // step_w):
            at = pl.ds(n * step_w, step_w)
            keep[s, :, at] = jnp.dot(
                hid[pl.ds(0, own_rows), :], wd[:, at], preferred_element_type=F32
            )

    for load in loads[1:]:
        load.wait()

    for wave in range(hops + chunks):
        for cc in range(chunks):
            h = wave + 1 - cc
            if 1 <= h <= hops:
                hop_out(cc, h)
            elif h == hops + 1:
                hop_last(cc)
        done = wave + 1 - hops - 1
        if 0 <= done < chunks:
            experts(done)

    order = list(range(1, chunks)) + [0]
    finished = set()
    back_sent = set()
    for h in range(1, hops + 1):
        for cc in order:
            ring_step(cc + 1, h)
    for cc in order:
        total = ring_end(cc + 1)
        span = TILE * folds
        for b in range(folds):
            fold[pl.ds(b, TILE, stride=folds), :] = total[
                :, b * LANES : (b + 1) * LANES
            ]
        bs[pl.ds(cc * span, span), :] = fold[pl.ds(0, span), :].astype(BF16)
        finished.add(cc)
        for p in range(1, n_sp):
            needs = {p * piece // span, ((p + 1) * piece - 1) // span}
            if p not in back_sent and needs <= finished:
                back_sent.add(p)
                z_start(1, bs, br, p)
    br[pl.ds(0, piece), :] = bs[pl.ds(0, piece), :]

    for p in range(1, n_sp):
        across[1, p].wait_recv()
    fold[...] = br[...].astype(F32)
    for b in range(folds):
        back[:, pl.ds(b * LANES, LANES)] = fold[
            pl.ds(b, slots, stride=folds), :
        ].astype(BF16)
    mix_w = mix_w[:, :slots]
    mix_hi = mix_w.astype(BF16)
    mix_lo = (mix_w - mix_hi.astype(F32)).astype(BF16)
    picked = back[...]
    combined = jnp.dot(mix_hi, picked, preferred_element_type=F32) + jnp.dot(
        mix_lo, picked, preferred_element_type=F32
    )
    out[...] = (stream_ref[...] + rms_scale(combined, gain_rows[2:3, :])).astype(BF16)

    for copy in pending:
        copy.wait_send()


def per_device(
    resid,
    gate_b,
    gate_c,
    value,
    taps,
    doc_ids,
    out_weight,
    norm_gains,
    routes,
    route_weights,
    w_gate,
    w_up,
    w_down,
):
    n_sp, n_tp = lax.axis_size("sp"), lax.axis_size("tp")
    tok, ch = gate_b.shape
    rows, width = resid.shape
    units = w_gate.shape[2]
    cap = max(2, 3 * TOP * rows // (2 * n_sp))
    chips = n_tp // 2
    hops = chips // 2
    slots = n_sp * cap
    chunks = slots // TILE
    folds = width // LANES
    sets = chunks + 1
    own_rows = chips * TILE
    ids = jnp.broadcast_to(doc_ids.astype(F32)[:, None], (tok, LANES))
    vmem = pl.BlockSpec(memory_space=pltpu.VMEM)
    hbm = pl.BlockSpec(memory_space=pl.ANY)
    dma = pltpu.SemaphoreType.DMA
    return pl.pallas_call(
        functools.partial(layer_kernel, n_sp, n_tp, cap),
        out_shape=jax.ShapeDtypeStruct((rows, width), BF16),
        in_specs=[vmem] * 6 + [hbm] + [vmem] * 3 + [hbm] * 3,
        out_specs=vmem,
        scratch_shapes=[
            pltpu.VMEM(out_weight.shape, BF16),
            pltpu.VMEM(w_gate.shape[1:], BF16),
            pltpu.VMEM(w_up.shape[1:], BF16),
            pltpu.VMEM(w_down.shape[1:], BF16),
            pltpu.VMEM((tok + 8, ch), F32),
            pltpu.VMEM((tok + 8, ch), F32),
            pltpu.VMEM((16, ch), F32),
            pltpu.VMEM((16, ch), F32),
            pltpu.VMEM((tok, ch), BF16),
            pltpu.VMEM((2, own_rows, ch), BF16),
            pltpu.VMEM((slots * folds, LANES), BF16),
            pltpu.VMEM((slots * folds, LANES), BF16),
            pltpu.VMEM((slots * folds, LANES), BF16),
            pltpu.VMEM((slots * folds, LANES), BF16),
            pltpu.VMEM((slots * folds, LANES), F32),
            pltpu.VMEM((chunks * n_tp * TILE, width), BF16),
            pltpu.VMEM((n_tp * TILE, units), BF16),
            pltpu.VMEM((sets, own_rows, width), BF16),
            pltpu.VMEM((sets, own_rows, width), BF16),
            pltpu.VMEM((sets, own_rows, width), F32),
            pltpu.VMEM((sets, chips, TILE, width), BF16),
            pltpu.VMEM((sets, hops, TILE, width), BF16),
            pltpu.VMEM((sets, hops, TILE, width), BF16),
            pltpu.VMEM((rows, width), F32),
            pltpu.VMEM((slots, width), BF16),
            dma((4,)),
            dma((2,)),
            dma((2, n_sp)),
            dma((2, n_sp)),
            dma((sets,)),
            dma((sets,)),
            dma((sets, hops)),
            dma((sets, hops)),
            dma((sets, hops)),
            dma((sets, hops)),
            dma((chunks, chips)),
            dma((chunks, chips)),
            dma((chunks, hops)),
            dma((chunks, hops)),
            dma((chunks, hops)),
            dma((chunks, hops)),
        ],
        compiler_params=pltpu.CompilerParams(
            collective_id=0,
            has_side_effects=True,
            vmem_limit_bytes=56 * 1024 * 1024,
        ),
        name="layer",
    )(
        resid,
        gate_b,
        gate_c,
        value,
        taps,
        ids,
        out_weight,
        norm_gains,
        routes,
        route_weights,
        w_gate,
        w_up,
        w_down,
    )


def solution(mesh):
    return jax.shard_map(
        per_device,
        mesh=mesh,
        in_specs=(
            P(("grp", "sp", "tp"), None),
            P(("grp", "sp"), "tp"),
            P(("grp", "sp"), "tp"),
            P(("grp", "sp"), "tp"),
            P(None, "tp"),
            P(("grp", "sp")),
            P("tp", None),
            P(),
            P(("grp", "sp"), None),
            P(("grp", "sp"), None),
            P("sp", None, "tp"),
            P("sp", None, "tp"),
            P("sp", "tp", None),
        ),
        out_specs=P(("grp", "sp", "tp"), None),
        check_vma=False,
    )
```

time: 294 us -> 138 us (0.47)
  waiting for transfers between devices: 150 us -> 0 us
  Pallas kernels: 0 us -> 133 us
  blocking collectives: 53.7 us -> 0 us
  starting transfers between devices: 32.9 us -> 0 us
  local copies, waits for them, and re-layouts: 21.9 us -> 3.8 us
  between operations: 13.6 us -> 0.01 us
  matrix products: 13.5 us -> 0 us
  other arithmetic: 6.01 us -> 0.68 us
    pallas_call x0 -> x1, Pallas kernels: none -> 133 us  [per_device(): pl.pallas_call(functools.partial(layer_kernel, n_sp, n_tp, cap), out_shap...]
    reduce_scatter x1 -> x0, waiting for transfers between devices: 66.9 us -> none  [per_device(): lax.psum_scatter(jnp.dot(block_rows, w_down[0], preferred_element_type=jn...]
    all_to_all x1 -> x0, blocking collectives: 53.7 us -> none  [per_device(): lax.all_to_all(outgoing, 'sp', split_axis=0, concat_axis=0, tiled=True)]
    all_gather x1 -> x0, waiting for transfers between devices: 42.3 us -> none  [per_device(): lax.all_gather(arrived[None], 'tp', axis=0, tiled=True)]
    all_to_all x2 -> x0, waiting for transfers between devices: 41 us -> none  [the longest x1 25.4 us: sent_and_summed(): lax.all_to_all(tiles, axis, split_axis=0, concat_axis=0, tiled=True)]
    all_to_all x2 -> x0, starting transfers between devices: 20.7 us -> none  [the longest x1 13.1 us: per_device(): lax.all_to_all(results, 'sp', split_axis=0, concat_axis=0, tiled=True)]
    dot_general x3 -> x0, matrix products: 13.5 us -> none  [the longest x1 7.08 us: per_device(): jnp.dot(block_rows, w_down[0], preferred_element_type=jnp.float32)]
    ppermute x2 -> x0, starting transfers between devices: 12 us -> none  [passed_along(): return lax.ppermute(block, axis, route)]
  transfers between devices with their start and end apart: 6 -> 0, of which waited for: 4 -> 0; matrix products, arithmetic and copies ran while one was open for 2% -> 0% of each run, Pallas kernels for 0% -> 0%
where the time goes in v1:
time: 138 us
  Pallas kernels  133 us (96%)
  local copies, waits for them, and re-layouts  3.8 us (3%)
    pallas_call x1, Pallas kernels, per_device(): pl.pallas_call(functools.partial(layer_kernel, n_sp, n_tp, cap), out_shap...  133 us
    unnamed x7, local copies, waits for them, and re-layouts  3.07 us

profile of v1, /device:TPU:80, one launch (start us, length us, event | category | flops | bytes accessed | tf_op | source)
XLA Modules:
  0.0 138.0 jit_solution(4740768995897452754)
XLA Ops:
  0.0 0.7 convert_element_type.3
  0.7 0.0 copy-start
  0.7 0.7 broadcast_in_dim.2.ids
  1.4 0.0 copy-done
  1.4 0.0 copy-start.1
  1.4 0.8 copy.14.routes
  2.2 0.0 copy-done.1
  2.2 0.8 copy.15.route_w
  3.0 133.5 %layer.1 = bf16[16,2048]{1,0:T(8,128)(2,1)} custom-call(bf16[16,2048]{1,0:T(8,128)(2,1)} %resid.1, bf16[256,128]{1,0:T(8,128)(2,1)} %gate_b.1, bf16[256,128]{1,0:T(8,128)(2,1)} %gate_c.1, bf16[256,128]{1,0:T(8,128)(2,1)} %value.1, bf16[3,128]{1,0:T(4,128)(2,1)} %taps.1, f32[256,128]{1,0:T(8,128)} %broadcast_in_dim.2.ids, bf16[128,2048]{1,0:T(8,128)(2,1)} %out_w.1, ...), custom_call_target="tpu_custom_call" | custom-call | tf_op jit(solution)/shard_map/layer/pallas_call | solution.py:467
  136.5 1.5 %copy.17 = bf16[16,2048]{1,0:T(8,128)(2,1)} copy(bf16[16,2048]{1,0:T(8,128)(2,1)} %layer.1) | data formatting | bytes 131072
Async XLA Ops:
  0.7 0.7 copy-start
  1.4 0.8 copy-start.1

commit v2 on v1

v2 whole, which is shorter than its diff:
```python
import functools

import jax
import jax.numpy as jnp
from jax import lax
from jax.experimental import pallas as pl
from jax.experimental.pallas import tpu as pltpu
from jax.sharding import PartitionSpec as P

TAPS = 3
TOP = 2
LANES = 128
TILE = 16

norm_eps = 1e-06
BF16 = jnp.bfloat16
F32 = jnp.float32
MESH = pl.DeviceIdType.MESH


def rms_scale(values, gain_row):
    mean_sq = jnp.mean(values * values, axis=-1, keepdims=True)
    return values * lax.rsqrt(mean_sq + norm_eps) * gain_row


def layer_kernel(
    n_sp,
    n_tp,
    cap,
    rings,
    resid_h,
    gate_b_h,
    gate_c_h,
    value_h,
    taps_h,
    ids_h,
    out_w_h,
    gains_h,
    routes_h,
    route_w_h,
    w_gate_h,
    w_up_h,
    w_down_h,
    out,
    resid,
    gate_b,
    gate_c,
    value,
    taps,
    ids,
    ow,
    gains,
    routes,
    route_w,
    wg,
    wu,
    wd,
    ext,
    ext_ids,
    halo_s,
    halo_r,
    mixed,
    sel,
    table,
    columns,
    zs,
    zr,
    bs,
    br,
    fold,
    xbuf,
    hid,
    pair_s,
    pair_r,
    keep,
    ring_s,
    ring_r,
    ring_l,
    stream_ref,
    back,
    load_sem,
    halo_sem,
    z_send,
    z_recv,
    back_recv,
    pair_send,
    pair_recv,
    ring_send,
    rr_recv,
    rl_recv,
    gather_send,
    d_recv,
    ar_recv,
    al_recv,
):
    tok, ch = gate_b.shape
    rows, width = resid.shape
    chips = n_tp // 2
    hops = chips // 2
    folds = width // LANES
    slots = n_sp * cap
    chunks = slots // TILE
    chunk_rows = n_tp * TILE
    own_rows = chips * TILE
    piece = cap * folds
    span = TILE * folds

    tp = lax.axis_index("tp")
    sp = lax.axis_index("sp")
    core = lax.rem(tp, 2)
    chip = lax.div(tp, 2)
    partner = {"tp": chip * 2 + (1 - core)}
    right = {"tp": lax.rem(chip + 1, chips) * 2 + core}
    left = {"tp": lax.rem(chip + chips - 1, chips) * 2 + core}

    def along(d):
        return {"sp": lax.rem(sp + d + n_sp, n_sp)}

    offs = [0] + [
        (p + 1) // 2 if p % 2 else -(p // 2) for p in range(1, n_sp)
    ]

    def pos_of(d):
        return next(p for p in range(n_sp) if (offs[p] - d) % n_sp == 0)

    def remote(src, dst, s_sem, r_sem, dev):
        return pltpu.make_async_remote_copy(
            src_ref=src,
            dst_ref=dst,
            send_sem=s_sem,
            recv_sem=r_sem,
            device_id=dev,
            device_id_type=MESH,
        )

    def send(src, dst, s_sem, r_sem, dev):
        copy = remote(src, dst, s_sem, r_sem, dev)
        copy.start()
        return copy

    def settle(ref, sem):
        pltpu.make_async_copy(ref, ref, sem).wait()

    barrier = pltpu.get_barrier_semaphore()
    greeted = [partner, right, left] + [along(d) for d in offs[1:]]
    for dev in greeted:
        pl.semaphore_signal(barrier, inc=1, device_id=dev, device_id_type=MESH)

    loads = {}
    for i, (name, src, dst) in enumerate(
        (
            ("ids", ids_h, ids),
            ("gate_c", gate_c_h, gate_c),
            ("value", value_h, value),
            ("gate_b", gate_b_h, gate_b),
            ("taps", taps_h, taps),
            ("ow", out_w_h, ow),
            ("routes", routes_h, routes),
            ("route_w", route_w_h, route_w),
            ("gains", gains_h, gains),
            ("resid", resid_h, resid),
            ("wg", w_gate_h.at[0], wg),
            ("wu", w_up_h.at[0], wu),
            ("wd", w_down_h.at[0], wd),
        )
    ):
        loads[name] = pltpu.make_async_copy(src, dst, load_sem.at[i])
        loads[name].start()

    parts = tok // LANES
    loads["ids"].wait()
    for k in range(parts):
        line = ids[k : k + 1, :].astype(F32)
        ext_ids[pl.ds(8 + k * LANES, LANES), :] = jnp.broadcast_to(
            line, (LANES, LANES)
        ).T
    loads["gate_c"].wait()
    loads["value"].wait()
    product = gate_c[...].astype(F32) * value[...].astype(F32)
    ext[pl.ds(8, tok), :] = product
    halo_s[pl.ds(0, 8), :] = product[tok - 8 :]
    halo_s[pl.ds(8, 8), :] = ext_ids[pl.ds(tok, 8), :]

    with jax.named_scope("barrier"):
        pl.semaphore_wait(barrier, len(greeted))
    halo = remote(halo_s, halo_r, halo_sem.at[0], halo_sem.at[1], along(1))

    @pl.when(sp < n_sp - 1)
    def _():
        halo.start()

    ext[pl.ds(0, 8), :] = jnp.zeros((8, ch), F32)
    ext_ids[pl.ds(0, 8), :] = jnp.full((8, LANES), -1.0, F32)
    loads["gate_b"].wait()
    loads["taps"].wait()

    @pl.when(sp > 0)
    def _():
        halo.wait_recv()
        ext[pl.ds(0, 8), :] = halo_r[pl.ds(0, 8), :]
        ext_ids[pl.ds(0, 8), :] = halo_r[pl.ds(8, 8), :]

    here = ext_ids[pl.ds(8, tok), :]
    tap_rows = taps[...].astype(F32)
    conv = tap_rows[0:1, :] * ext[pl.ds(8, tok), :]
    for lag in range(1, TAPS):
        same = ext_ids[pl.ds(8 - lag, tok), :] == here
        conv = conv + jnp.where(
            same, tap_rows[lag : lag + 1, :] * ext[pl.ds(8 - lag, tok), :], 0.0
        )
    mixed[...] = (gate_b[...].astype(F32) * conv).astype(BF16)

    def place(owner, o):
        block = lax.rem(chip + o, chips) * 2 + owner
        return pl.ds(pl.multiple_of(block * rows, rows), rows)

    for o in range(chips):
        sel[0, pl.ds(o * rows, rows), :] = mixed[place(core, o), :]
        sel[1, pl.ds(o * rows, rows), :] = mixed[place(1 - core, o), :]

    ring = {}

    def pair_start(k):
        s, at, cols = rings[k]
        at = pl.ds(at, cols)
        ring[k, "pair"] = send(
            pair_s.at[s, :, at],
            pair_r.at[s, :, at],
            pair_send.at[0],
            pair_recv.at[k],
            partner,
        )

    def ring_step(k, h):
        with jax.named_scope(f"rs{k}_{h}"):
            ring_hop(k, h)

    def ring_hop(k, h):
        s, at, cols = rings[k]
        all_c = pl.ds(at, cols)
        lo, hi = pl.ds(at, cols // 2), pl.ds(at + cols // 2, cols // 2)

        def share(o, c):
            r = pl.ds(o * TILE, TILE)
            return keep[s, r, c] + pair_r[s, r, c].astype(F32)

        if h == 1:
            ring[k, "pair"].wait_recv()
            ring_s[s, hops, :, all_c] = share(hops, all_c).astype(BF16)
        for name, buf, sem, dev, early, late in (
            ("r", ring_r, rr_recv, right, lo, hi),
            ("l", ring_l, rl_recv, left, hi, lo),
        ):
            o = hops + 1 - h
            if name == "l":
                o = (chips - o) % chips
            if h > 1:
                ring[k, name, h - 1].wait_recv()
            if h == 2:
                ring_s[s, o, :, early] = (
                    share(o, early) + buf[s, 0, :, early].astype(F32)
                ).astype(BF16)
                ring_s[s, o, :, late] = share(o, late).astype(BF16)
            elif h > 2:
                ring_s[s, o, :, all_c] = (
                    share(o, all_c) + buf[s, h - 2, :, all_c].astype(F32)
                ).astype(BF16)
            c = early if h == 1 else all_c
            ring[k, name, h] = send(
                ring_s.at[s, o, :, c],
                buf.at[s, h - 1, :, c],
                ring_send.at[0],
                sem.at[k, h - 1],
                dev,
            )

    def ring_end(k):
        with jax.named_scope(f"re{k}"):
            s, at, cols = rings[k]
            c = pl.ds(at, cols)
            ring[k, "r", hops].wait_recv()
            ring[k, "l", hops].wait_recv()
            return (
                keep[s, pl.ds(0, TILE), c]
                + pair_r[s, pl.ds(0, TILE), c].astype(F32)
                + ring_r[s, hops - 1, :, c].astype(F32)
                + ring_l[s, hops - 1, :, c].astype(F32)
            )

    first_rings = [k for k in range(len(rings)) if rings[k][0] == 0]
    loads["ow"].wait()
    step_w = min(512, width)
    for k in first_rings:
        _, at, cols = rings[k]
        for n in range(cols // step_w):
            c = pl.ds(at + n * step_w, step_w)
            pair_s[0, :, c] = jnp.dot(
                sel[1], ow[:, c], preferred_element_type=F32
            ).astype(BF16)
        pair_start(k)
    for n in range(width // step_w):
        c = pl.ds(n * step_w, step_w)
        keep[0, :, c] = jnp.dot(sel[0], ow[:, c], preferred_element_type=F32)
    for h in range(1, hops + 1):
        for k in first_rings:
            ring_step(k, h)

    loads["routes"].wait()
    loads["route_w"].wait()
    for k in range(TOP):
        for part in range(parts):
            c = pl.ds(part * LANES, LANES)
            table[pl.ds(k * parts + part, 1), :] = routes[pl.ds(k, 1), c].astype(F32)
            table[pl.ds((TOP + k) * parts + part, 1), :] = route_w[pl.ds(k, 1), c]
    columns[:, pl.ds(0, 2 * TOP * parts)] = table[...].T
    base = tp * rows
    my_part = lax.div(base, LANES)
    mine = columns[pl.ds(pl.multiple_of(base - my_part * LANES, rows), rows), :]

    def column(n):
        found = mine[:, n * parts : n * parts + 1]
        for part in range(1, parts):
            found = jnp.where(
                my_part == part, mine[:, n * parts + part : n * parts + part + 1], found
            )
        return found

    lane = lax.broadcasted_iota(jnp.int32, (rows, LANES), 1)
    pos = jnp.floor((lane.astype(F32) + 0.5) * (1.0 / cap)).astype(jnp.int32)
    depth = (lane - pos * cap).astype(F32)
    reach = (pos + 1) >> 1
    away = sp + jnp.where((pos & 1) == 1, reach, -reach)
    away = jnp.where(away < 0, away + n_sp, away)
    away = jnp.where(away >= n_sp, away - n_sp, away)
    expert = jnp.where(lane < slots, away, -1).astype(F32)
    first = (column(0) == expert).astype(F32)
    second = (column(1) == expert).astype(F32)
    named = first + second
    r_at = lax.broadcasted_iota(jnp.int32, (rows, rows), 0)
    c_at = lax.broadcasted_iota(jnp.int32, (rows, rows), 1)
    earlier = (c_at < r_at).astype(F32).astype(BF16)
    rank = jnp.dot(earlier, named.astype(BF16), preferred_element_type=F32)
    hit = named * (rank == depth).astype(F32)
    w_first, w_second = column(TOP), column(TOP + 1)
    w_sum = w_first + w_second
    mix_w = hit * (first * (w_first / w_sum) + second * (w_second / w_sum))
    pick = hit.T.astype(BF16)[:slots, :]

    loads["gains"].wait()
    loads["resid"].wait()
    gain_rows = gains[...]
    projected = jnp.concatenate([ring_end(k) for k in first_rings], axis=1)
    stream = resid[...].astype(F32) + rms_scale(projected, gain_rows[0:1, :])
    stream_ref[...] = stream
    normed = rms_scale(stream, gain_rows[1:2, :]).astype(BF16)

    outgoing = jnp.dot(pick, normed, preferred_element_type=F32)
    for b in range(folds):
        fold[pl.ds(b, slots, stride=folds), :] = outgoing[
            :, b * LANES : (b + 1) * LANES
        ]
    folded = fold[...].astype(BF16)
    zs[...] = folded
    zr[pl.ds(0, piece), :] = folded[:piece]

    group_of = [(p * piece) // span for p in range(n_sp)]

    def z_start(way, src, dst, p):
        q = pos_of(-offs[p])
        sem = z_recv.at[group_of[q]] if way == 0 else back_recv.at[0]
        send(
            src.at[pl.ds(p * piece, piece), :],
            dst.at[pl.ds(q * piece, piece), :],
            z_send.at[way],
            sem,
            along(offs[p]),
        )

    for p in reversed(range(1, n_sp)):
        z_start(0, zs, zr, p)

    gather = {}
    came = set()

    def block(cc, other, o):
        return pl.ds(cc * chunk_rows + other * own_rows + (o % chips) * TILE, TILE)

    def to_partner(cc, o):
        send(
            xbuf.at[block(cc, 0, o), :],
            xbuf.at[block(cc, 1, o), :],
            gather_send.at[0],
            d_recv.at[cc],
            partner,
        )

    def hop_out(cc, h):
        with jax.named_scope(f"ag{cc}_{h}"):
            gather_hop(cc, h)

    def gather_hop(cc, h):
        if h == 1:
            for g in range(cc + 1):
                here_p = [p for p in range(1, n_sp) if group_of[p] == g]
                if g not in came and here_p[0] * piece < (cc + 1) * span and (
                    (here_p[-1] + 1) * piece > cc * span
                ):
                    came.add(g)
                    settle(
                        zr.at[pl.ds(here_p[0] * piece, len(here_p) * piece), :],
                        z_recv.at[g],
                    )
            fold[pl.ds(0, span), :] = zr[pl.ds(cc * span, span), :].astype(F32)
            for b in range(folds):
                xbuf[block(cc, 0, 0), pl.ds(b * LANES, LANES)] = fold[
                    pl.ds(b, TILE, stride=folds), :
                ].astype(BF16)
        else:
            gather[cc, "r", h - 1].wait_recv()
            gather[cc, "l", h - 1].wait_recv()
        for name, sign, dev, sem, at in (
            ("r", -1, right, ar_recv, 0),
            ("l", 1, left, al_recv, width // 2),
        ):
            c = pl.ds(at, width // 2) if h == hops else slice(None)
            gather[cc, name, h] = send(
                xbuf.at[block(cc, 0, sign * (h - 1)), c],
                xbuf.at[block(cc, 0, sign * h), c],
                gather_send.at[0],
                sem.at[cc, h - 1],
                dev,
            )
        to_partner(cc, 1 - h)
        if h > 1:
            to_partner(cc, h - 1)

    def hop_last(cc):
        with jax.named_scope(f"agl{cc}"):
            gather[cc, "r", hops].wait_recv()
            gather[cc, "l", hops].wait_recv()
            to_partner(cc, hops)

    def experts(cc):
        s = cc + 1
        k = next(k for k in range(len(rings)) if rings[k][0] == s)
        with jax.named_scope(f"exw{cc}"):
            settle(
                xbuf.at[pl.ds(cc * chunk_rows + own_rows, own_rows), :], d_recv.at[cc]
            )
        with jax.named_scope(f"exc{cc}"):
            x = xbuf[pl.ds(cc * chunk_rows, chunk_rows), :]
            g = jnp.dot(x, wg[...], preferred_element_type=F32)
            u = jnp.dot(x, wu[...], preferred_element_type=F32)
            hid[...] = (g / (1.0 + jnp.exp(-g)) * u).astype(BF16)
            for n in range(width // step_w):
                c = pl.ds(n * step_w, step_w)
                pair_s[s, :, c] = jnp.dot(
                    hid[pl.ds(own_rows, own_rows), :],
                    wd[:, c],
                    preferred_element_type=F32,
                ).astype(BF16)
            pair_start(k)
            for n in range(width // step_w):
                c = pl.ds(n * step_w, step_w)
                keep[s, :, c] = jnp.dot(
                    hid[pl.ds(0, own_rows), :], wd[:, c], preferred_element_type=F32
                )
        return k

    order = list(reversed(range(chunks)))
    for h in range(1, hops + 1):
        for cc in order:
            hop_out(cc, h)
    for name in ("wg", "wu", "wd"):
        loads[name].wait()
    ring_of = {}
    for i, cc in enumerate(order):
        if i == 0:
            hop_last(cc)
        if i + 1 < chunks:
            hop_last(order[i + 1])
        ring_of[cc] = experts(cc)
        if i > 0:
            ring_step(ring_of[order[i - 1]], 1)
    ring_step(ring_of[order[-1]], 1)
    for h in range(2, hops + 1):
        for cc in order:
            ring_step(ring_of[cc], h)

    finished = set()
    back_sent = set()
    for cc in order:
        total = ring_end(ring_of[cc])
        for b in range(folds):
            fold[pl.ds(b, TILE, stride=folds), :] = total[
                :, b * LANES : (b + 1) * LANES
            ]
        bs[pl.ds(cc * span, span), :] = fold[pl.ds(0, span), :].astype(BF16)
        finished.add(cc)
        for p in reversed(range(1, n_sp)):
            needs = {p * piece // span, ((p + 1) * piece - 1) // span}
            if p not in back_sent and needs <= finished:
                back_sent.add(p)
                z_start(1, bs, br, p)
    br[pl.ds(0, piece), :] = bs[pl.ds(0, piece), :]

    far = (n_sp - 1) * piece
    ring_rows = (2 * hops - 1) * TILE
    with jax.named_scope("sendwait"):
        settle(pair_s, pair_send.at[0])
        settle(pair_s.at[:, pl.ds(0, ring_rows), :], ring_send.at[0])
        settle(
            xbuf.at[pl.ds(0, chunks * (ring_rows + own_rows)), :], gather_send.at[0]
        )
        settle(zs.at[pl.ds(piece, far), :], z_send.at[0])

        @pl.when(sp < n_sp - 1)
        def _():
            halo.wait_send()

    with jax.named_scope("backwait"):
        settle(br.at[pl.ds(piece, far), :], back_recv.at[0])
    fold[...] = br[...].astype(F32)
    for b in range(folds):
        back[:, pl.ds(b * LANES, LANES)] = fold[
            pl.ds(b, slots, stride=folds), :
        ].astype(BF16)
    mix_w = mix_w[:, :slots]
    mix_hi = mix_w.astype(BF16)
    mix_lo = (mix_w - mix_hi.astype(F32)).astype(BF16)
    picked = back[...]
    combined = jnp.dot(mix_hi, picked, preferred_element_type=F32) + jnp.dot(
        mix_lo, picked, preferred_element_type=F32
    )
    out[...] = stream_ref[...] + rms_scale(combined, gain_rows[2:3, :])
    settle(bs.at[pl.ds(piece, far), :], z_send.at[1])


def per_device(
    resid,
    gate_b,
    gate_c,
    value,
    taps,
    doc_ids,
    out_weight,
    norm_gains,
    routes,
    route_weights,
    w_gate,
    w_up,
    w_down,
):
    n_sp, n_tp = lax.axis_size("sp"), lax.axis_size("tp")
    tok, ch = gate_b.shape
    rows, width = resid.shape
    units = w_gate.shape[2]
    cap = max(2, 3 * TOP * rows // (2 * n_sp))
    chips = n_tp // 2
    hops = chips // 2
    slots = n_sp * cap
    chunks = slots // TILE
    folds = width // LANES
    sets = chunks + 1
    own_rows = chips * TILE
    parts = tok // LANES
    rings = [(0, 0, width // 2), (0, width // 2, width // 2)]
    rings += [(s, 0, width) for s in range(1, sets)]
    n_rings = len(rings)
    operands = (
        resid,
        gate_b,
        gate_c,
        value,
        taps,
        doc_ids.reshape(parts, LANES),
        out_weight,
        norm_gains,
        routes.T,
        route_weights.T,
        w_gate,
        w_up,
        w_down,
    )
    hbm = pl.BlockSpec(memory_space=pl.ANY)
    vmem = pltpu.VMEM
    dma = pltpu.SemaphoreType.DMA
    result = pl.pallas_call(
        functools.partial(layer_kernel, n_sp, n_tp, cap, rings),
        out_shape=jax.ShapeDtypeStruct((rows, width), F32),
        in_specs=[hbm] * len(operands),
        out_specs=pl.BlockSpec(memory_space=vmem),
        scratch_shapes=[
            *[vmem(a.shape, a.dtype) for a in operands[:10]],
            *[vmem(a.shape[1:], a.dtype) for a in operands[10:]],
            vmem((tok + 8, ch), F32),
            vmem((tok + 8, LANES), F32),
            vmem((16, ch), F32),
            vmem((16, ch), F32),
            vmem((tok, ch), BF16),
            vmem((2, own_rows, ch), BF16),
            vmem((2 * TOP * parts, LANES), F32),
            vmem((LANES, LANES), F32),
            vmem((slots * folds, LANES), BF16),
            vmem((slots * folds, LANES), BF16),
            vmem((slots * folds, LANES), BF16),
            vmem((slots * folds, LANES), BF16),
            vmem((slots * folds, LANES), F32),
            vmem((chunks * n_tp * TILE, width), BF16),
            vmem((n_tp * TILE, units), BF16),
            vmem((sets, own_rows, width), BF16),
            vmem((sets, own_rows, width), BF16),
            vmem((sets, own_rows, width), F32),
            vmem((sets, chips, TILE, width), BF16),
            vmem((sets, hops, TILE, width), BF16),
            vmem((sets, hops, TILE, width), BF16),
            vmem((rows, width), F32),
            vmem((slots, width), BF16),
            dma((len(operands),)),
            dma((2,)),
            dma((2,)),
            dma((chunks,)),
            dma((1,)),
            dma((1,)),
            dma((n_rings,)),
            dma((1,)),
            dma((n_rings, hops)),
            dma((n_rings, hops)),
            dma((1,)),
            dma((chunks,)),
            dma((chunks, hops)),
            dma((chunks, hops)),
        ],
        compiler_params=pltpu.CompilerParams(
            collective_id=0,
            has_side_effects=True,
            vmem_limit_bytes=56 * 1024 * 1024,
        ),
        name="layer",
    )(*operands)
    return result.astype(BF16)


def solution(mesh):
    return jax.shard_map(
        per_device,
        mesh=mesh,
        in_specs=(
            P(("grp", "sp", "tp"), None),
            P(("grp", "sp"), "tp"),
            P(("grp", "sp"), "tp"),
            P(("grp", "sp"), "tp"),
            P(None, "tp"),
            P(("grp", "sp")),
            P("tp", None),
            P(),
            P(("grp", "sp"), None),
            P(("grp", "sp"), None),
            P("sp", None, "tp"),
            P("sp", None, "tp"),
            P("sp", "tp", None),
        ),
        out_specs=P(("grp", "sp", "tp"), None),
        check_vma=False,
    )
```

time: 138 us -> 128 us (0.928)
  Pallas kernels: 133 us -> 127 us
  local copies, waits for them, and re-layouts: 3.8 us -> 0 us
    pallas_call x1, Pallas kernels: 133 us -> 127 us  [per_device(): pl.pallas_call(functools.partial(layer_kernel, n_sp, n_tp, cap, rings), o...]
    unnamed x7 -> x0, local copies, waits for them, and re-layouts: 3.07 us -> none
where the time goes in v2:
time: 128 us
  Pallas kernels  127 us (99%)
  other arithmetic  1.54 us (1%)
    pallas_call x1, Pallas kernels, per_device(): pl.pallas_call(functools.partial(layer_kernel, n_sp, n_tp, cap, rings), o...  127 us

profile of v2, /device:TPU:80, one launch (start us, length us, event | category | flops | bytes accessed | tf_op | source)
XLA Modules:
  0.0 128.3 jit_solution(11650031768653500457)
XLA Ops:
  0.0 126.8 %layer.1 = f32[16,2048]{1,0:T(8,128)} custom-call(bf16[16,2048]{1,0:T(8,128)(2,1)} %resid_h.1, bf16[256,128]{1,0:T(8,128)(2,1)} %gate_b_h.1, bf16[256,128]{1,0:T(8,128)(2,1)} %gate_c_h.1, bf16[256,128]{1,0:T(8,128)(2,1)} %value_h.1, bf16[3,128]{1,0:T(4,128)(2,1)} %taps_h.1, s32[2,128]{1,0:T(2,128)} %bitcast.5, bf16[128,2048]{1,0:T(8,128)(2,1)} %out_w_h.1, ...), custom_call_target="tpu_custom_call" | custom-call | tf_op jit(solution)/shard_map/layer/pallas_call | solution.py:588
  126.8 1.5 %convert_element_type.3 = bf16[16,2048]{1,0:T(8,128)(2,1)} convert(f32[16,2048]{1,0:T(8,128)} %layer.1) | non-fusion elementwise | flops 32768 | bytes 196608 | tf_op jit(solution)/shard_map/convert_element_type | solution.py:641

commit v3 on v2

--- a/solution.py
+++ b/solution.py
@@ -13,6 +13,22 @@
 TILE = 16
 
 norm_eps = 1e-06
+
+ORDER = (
+    (0, 0, 0, 1), (0, 0, 1, 1), (0, 1, 0, 1), (0, 1, 1, 1), (0, 0, 0, 2),
+    (0, 0, 1, 2), (0, 1, 0, 2), (0, 1, 1, 2), (0, 0, 0, 3), (0, 0, 1, 3),
+    (0, 1, 0, 3), (0, 2, 0, 1), (0, 2, 1, 1), (0, 0, 0, 4), (0, 1, 1, 3),
+    (0, 0, 1, 4), (0, 1, 0, 4), (0, 2, 0, 2), (0, 2, 1, 2), (4, 0, 0),
+    (4, 0, 1), (4, 1, 0), (0, 2, 0, 3), (0, 2, 1, 3), (0, 1, 1, 4),
+    (1, 0), (0, 2, 0, 4), (0, 2, 1, 4), (4, 1, 1), (2, 0, 0, 1),
+    (2, 0, 1, 1), (4, 2, 0), (4, 2, 1), (2, 0, 0, 2), (2, 0, 1, 2),
+    (1, 2), (1, 1), (2, 2, 0, 1), (2, 2, 1, 1), (2, 1, 0, 1),
+    (2, 1, 1, 1), (2, 0, 0, 3), (2, 0, 1, 3), (2, 2, 0, 2), (2, 2, 1, 2),
+    (2, 1, 0, 2), (2, 1, 1, 2), (2, 0, 0, 4), (2, 2, 0, 3), (2, 2, 1, 3),
+    (2, 1, 0, 3), (2, 1, 1, 3), (3, 0, 0), (2, 2, 0, 4), (2, 2, 1, 4),
+    (2, 1, 0, 4), (2, 1, 1, 4), (2, 0, 1, 4), (3, 2, 0), (3, 2, 1),
+    (3, 1, 0), (3, 1, 1), (3, 0, 1),
+)
 BF16 = jnp.bfloat16
 F32 = jnp.float32
 MESH = pl.DeviceIdType.MESH
@@ -80,6 +96,8 @@
     back,
     load_sem,
     halo_sem,
+    below_sem,
+    above_sem,
     z_send,
     z_recv,
     back_recv,
@@ -116,13 +134,6 @@
     def along(d):
         return {"sp": lax.rem(sp + d + n_sp, n_sp)}
 
-    offs = [0] + [
-        (p + 1) // 2 if p % 2 else -(p // 2) for p in range(1, n_sp)
-    ]
-
-    def pos_of(d):
-        return next(p for p in range(n_sp) if (offs[p] - d) % n_sp == 0)
-
     def remote(src, dst, s_sem, r_sem, dev):
         return pltpu.make_async_remote_copy(
             src_ref=src,
@@ -142,9 +153,18 @@
         pltpu.make_async_copy(ref, ref, sem).wait()
 
     barrier = pltpu.get_barrier_semaphore()
-    greeted = [partner, right, left] + [along(d) for d in offs[1:]]
+    greeted = [partner, right, left]
     for dev in greeted:
         pl.semaphore_signal(barrier, inc=1, device_id=dev, device_id_type=MESH)
+    has_below, has_above = sp > 0, sp < n_sp - 1
+
+    @pl.when(has_below)
+    def _():
+        pl.semaphore_signal(barrier, inc=1, device_id=along(-1), device_id_type=MESH)
+
+    @pl.when(has_above)
+    def _():
+        pl.semaphore_signal(barrier, inc=1, device_id=along(1), device_id_type=MESH)
 
     loads = {}
     for i, (name, src, dst) in enumerate(
@@ -182,10 +202,13 @@
     halo_s[pl.ds(8, 8), :] = ext_ids[pl.ds(tok, 8), :]
 
     with jax.named_scope("barrier"):
-        pl.semaphore_wait(barrier, len(greeted))
+        pl.semaphore_wait(
+            barrier,
+            len(greeted) + jnp.where(has_below, 1, 0) + jnp.where(has_above, 1, 0),
+        )
     halo = remote(halo_s, halo_r, halo_sem.at[0], halo_sem.at[1], along(1))
 
-    @pl.when(sp < n_sp - 1)
+    @pl.when(has_above)
     def _():
         halo.start()
 
@@ -194,11 +217,29 @@
     loads["gate_b"].wait()
     loads["taps"].wait()
 
-    @pl.when(sp > 0)
+    @pl.when(has_below)
     def _():
         halo.wait_recv()
         ext[pl.ds(0, 8), :] = halo_r[pl.ds(0, 8), :]
         ext_ids[pl.ds(0, 8), :] = halo_r[pl.ds(8, 8), :]
+
+    @pl.when(has_below)
+    def _():
+        pl.semaphore_wait(below_sem, 1)
+
+    @pl.when(has_above)
+    def _():
+        pl.semaphore_signal(
+            below_sem, inc=1, device_id=along(1), device_id_type=MESH
+        )
+
+    for d in range(1, n_sp):
+
+        @pl.when(sp >= d)
+        def _():
+            pl.semaphore_signal(
+                above_sem, inc=1, device_id=along(-d), device_id_type=MESH
+            )
 
     here = ext_ids[pl.ds(8, tok), :]
     tap_rows = taps[...].astype(F32)
@@ -287,7 +328,10 @@
                 + ring_l[s, hops - 1, :, c].astype(F32)
             )
 
-    first_rings = [k for k in range(len(rings)) if rings[k][0] == 0]
+    set_rings = {}
+    for k, (s, _, _) in enumerate(rings):
+        set_rings.setdefault(s, []).append(k)
+    first_rings = set_rings[0]
     loads["ow"].wait()
     step_w = min(512, width)
     for k in first_rings:
@@ -328,11 +372,7 @@
     lane = lax.broadcasted_iota(jnp.int32, (rows, LANES), 1)
     pos = jnp.floor((lane.astype(F32) + 0.5) * (1.0 / cap)).astype(jnp.int32)
     depth = (lane - pos * cap).astype(F32)
-    reach = (pos + 1) >> 1
-    away = sp + jnp.where((pos & 1) == 1, reach, -reach)
-    away = jnp.where(away < 0, away + n_sp, away)
-    away = jnp.where(away >= n_sp, away - n_sp, away)
-    expert = jnp.where(lane < slots, away, -1).astype(F32)
+    expert = jnp.where(lane < slots, pos, -1).astype(F32)
     first = (column(0) == expert).astype(F32)
     second = (column(1) == expert).astype(F32)
     named = first + second
@@ -361,23 +401,25 @@
         ]
     folded = fold[...].astype(BF16)
     zs[...] = folded
-    zr[pl.ds(0, piece), :] = folded[:piece]
-
-    group_of = [(p * piece) // span for p in range(n_sp)]
-
-    def z_start(way, src, dst, p):
-        q = pos_of(-offs[p])
-        sem = z_recv.at[group_of[q]] if way == 0 else back_recv.at[0]
+    my_piece = pl.ds(pl.multiple_of(sp * piece, piece), piece)
+    zr[my_piece, :] = zs[my_piece, :]
+
+    with jax.named_scope("above"):
+
+        @pl.when(has_above)
+        def _():
+            pl.semaphore_wait(above_sem, n_sp - 1 - sp)
+
+    for p in range(1, n_sp):
+        d = (p + 1) // 2 if p % 2 else -(p // 2)
+        there = lax.rem(sp + d + n_sp, n_sp)
         send(
-            src.at[pl.ds(p * piece, piece), :],
-            dst.at[pl.ds(q * piece, piece), :],
-            z_send.at[way],
-            sem,
-            along(offs[p]),
-        )
-
-    for p in reversed(range(1, n_sp)):
-        z_start(0, zs, zr, p)
+            zs.at[pl.ds(pl.multiple_of(there * piece, piece), piece), :],
+            zr.at[my_piece, :],
+            z_send.at[0],
+            z_recv.at[sp],
+            {"sp": there},
+        )
 
     gather = {}
     came = set()
@@ -385,64 +427,68 @@
     def block(cc, other, o):
         return pl.ds(cc * chunk_rows + other * own_rows + (o % chips) * TILE, TILE)
 
-    def to_partner(cc, o):
+    part_w = width // 2
+
+    def to_partner(cc, part, o):
+        c = pl.ds(part * part_w, part_w)
         send(
-            xbuf.at[block(cc, 0, o), :],
-            xbuf.at[block(cc, 1, o), :],
+            xbuf.at[block(cc, 0, o), c],
+            xbuf.at[block(cc, 1, o), c],
             gather_send.at[0],
             d_recv.at[cc],
             partner,
         )
 
-    def hop_out(cc, h):
-        with jax.named_scope(f"ag{cc}_{h}"):
-            gather_hop(cc, h)
-
-    def gather_hop(cc, h):
-        if h == 1:
-            for g in range(cc + 1):
-                here_p = [p for p in range(1, n_sp) if group_of[p] == g]
-                if g not in came and here_p[0] * piece < (cc + 1) * span and (
-                    (here_p[-1] + 1) * piece > cc * span
-                ):
-                    came.add(g)
-                    settle(
-                        zr.at[pl.ds(here_p[0] * piece, len(here_p) * piece), :],
-                        z_recv.at[g],
-                    )
-            fold[pl.ds(0, span), :] = zr[pl.ds(cc * span, span), :].astype(F32)
+    def gather_hop(cc, part, h):
+        with jax.named_scope(f"ag{cc}{part}{h}"):
+            gather_step(cc, part, h)
+
+    def arrive(src):
+        @pl.when(sp != src)
+        def _():
+            settle(zr.at[pl.ds(src * piece, piece), :], z_recv.at[src])
+
+    def gather_step(cc, part, h):
+        if h == 1 and part == 0:
+            for src in range(n_sp):
+                if src not in came and src * piece < (cc + 1) * span:
+                    came.add(src)
+                    arrive(src)
+            fold[pl.ds(cc * span, span), :] = zr[pl.ds(cc * span, span), :].astype(F32)
             for b in range(folds):
                 xbuf[block(cc, 0, 0), pl.ds(b * LANES, LANES)] = fold[
-                    pl.ds(b, TILE, stride=folds), :
+                    pl.ds(cc * span + b, TILE, stride=folds), :
                 ].astype(BF16)
-        else:
-            gather[cc, "r", h - 1].wait_recv()
-            gather[cc, "l", h - 1].wait_recv()
-        for name, sign, dev, sem, at in (
+        elif h > 1:
+            gather[cc, part, "r", h - 1].wait_recv()
+            gather[cc, part, "l", h - 1].wait_recv()
+        k = cc * 2 + part
+        for name, sign, dev, sem, half in (
             ("r", -1, right, ar_recv, 0),
-            ("l", 1, left, al_recv, width // 2),
+            ("l", 1, left, al_recv, 1),
         ):
-            c = pl.ds(at, width // 2) if h == hops else slice(None)
-            gather[cc, name, h] = send(
+            c = pl.ds(part * part_w, part_w)
+            if h == hops:
+                c = pl.ds(part * part_w + half * (part_w // 2), part_w // 2)
+            gather[cc, part, name, h] = send(
                 xbuf.at[block(cc, 0, sign * (h - 1)), c],
                 xbuf.at[block(cc, 0, sign * h), c],
                 gather_send.at[0],
-                sem.at[cc, h - 1],
+                sem.at[k, h - 1],
                 dev,
             )
-        to_partner(cc, 1 - h)
+        to_partner(cc, part, 1 - h)
         if h > 1:
-            to_partner(cc, h - 1)
-
-    def hop_last(cc):
-        with jax.named_scope(f"agl{cc}"):
-            gather[cc, "r", hops].wait_recv()
-            gather[cc, "l", hops].wait_recv()
-            to_partner(cc, hops)
+            to_partner(cc, part, h - 1)
+
+    def gather_last(cc, part):
+        with jax.named_scope(f"al{cc}{part}"):
+            gather[cc, part, "r", hops].wait_recv()
+            gather[cc, part, "l", hops].wait_recv()
+            to_partner(cc, part, hops)
 
     def experts(cc):
         s = cc + 1
-        k = next(k for k in range(len(rings)) if rings[k][0] == s)
         with jax.named_scope(f"exw{cc}"):
             settle(
                 xbuf.at[pl.ds(cc * chunk_rows + own_rows, own_rows), :], d_recv.at[cc]
@@ -459,50 +505,61 @@
                     wd[:, c],
                     preferred_element_type=F32,
                 ).astype(BF16)
-            pair_start(k)
+            for k in set_rings[s]:
+                pair_start(k)
             for n in range(width // step_w):
                 c = pl.ds(n * step_w, step_w)
                 keep[s, :, c] = jnp.dot(
                     hid[pl.ds(0, own_rows), :], wd[:, c], preferred_element_type=F32
                 )
-        return k
-
-    order = list(reversed(range(chunks)))
-    for h in range(1, hops + 1):
-        for cc in order:
-            hop_out(cc, h)
-    for name in ("wg", "wu", "wd"):
-        loads[name].wait()
-    ring_of = {}
-    for i, cc in enumerate(order):
-        if i == 0:
-            hop_last(cc)
-        if i + 1 < chunks:
-            hop_last(order[i + 1])
-        ring_of[cc] = experts(cc)
-        if i > 0:
-            ring_step(ring_of[order[i - 1]], 1)
-    ring_step(ring_of[order[-1]], 1)
-    for h in range(2, hops + 1):
-        for cc in order:
-            ring_step(ring_of[cc], h)
 
     finished = set()
     back_sent = set()
-    for cc in order:
-        total = ring_end(ring_of[cc])
-        for b in range(folds):
-            fold[pl.ds(b, TILE, stride=folds), :] = total[
+    ended = {}
+
+    def finish(cc, part):
+        k = set_rings[cc + 1][part]
+        total = ring_end(k)
+        first_fold = rings[k][1] // LANES
+        for b in range(rings[k][2] // LANES):
+            fold[pl.ds(cc * span + first_fold + b, TILE, stride=folds), :] = total[
                 :, b * LANES : (b + 1) * LANES
             ]
-        bs[pl.ds(cc * span, span), :] = fold[pl.ds(0, span), :].astype(BF16)
+        ended[cc] = ended.get(cc, 0) + 1
+        if ended[cc] < len(set_rings[cc + 1]):
+            return
+        at = pl.ds(cc * span, span)
+        bs[at, :] = fold[at, :].astype(BF16)
         finished.add(cc)
-        for p in reversed(range(1, n_sp)):
+        for p in range(n_sp):
             needs = {p * piece // span, ((p + 1) * piece - 1) // span}
             if p not in back_sent and needs <= finished:
                 back_sent.add(p)
-                z_start(1, bs, br, p)
-    br[pl.ds(0, piece), :] = bs[pl.ds(0, piece), :]
+
+                @pl.when(sp != p)
+                def _():
+                    send(
+                        bs.at[pl.ds(p * piece, piece), :],
+                        br.at[my_piece, :],
+                        z_send.at[1],
+                        back_recv.at[0],
+                        {"sp": p},
+                    )
+
+    for name in ("wg", "wu", "wd"):
+        loads[name].wait()
+    for op in ORDER:
+        if op[0] == 0:
+            gather_hop(*op[1:])
+        elif op[0] == 4:
+            gather_last(*op[1:])
+        elif op[0] == 1:
+            experts(*op[1:])
+        elif op[0] == 2:
+            ring_step(set_rings[op[1] + 1][op[2]], op[3])
+        else:
+            finish(*op[1:])
+    br[my_piece, :] = bs[my_piece, :]
 
     far = (n_sp - 1) * piece
     ring_rows = (2 * hops - 1) * TILE
@@ -514,7 +571,7 @@
         )
         settle(zs.at[pl.ds(piece, far), :], z_send.at[0])
 
-        @pl.when(sp < n_sp - 1)
+        @pl.when(has_above)
         def _():
             halo.wait_send()
 
@@ -564,8 +621,9 @@
     sets = chunks + 1
     own_rows = chips * TILE
     parts = tok // LANES
-    rings = [(0, 0, width // 2), (0, width // 2, width // 2)]
-    rings += [(s, 0, width) for s in range(1, sets)]
+    rings = [(0, k * (width // 4), width // 4) for k in range(4)]
+    for s in range(1, sets):
+        rings += [(s, k * (width // 2), width // 2) for k in range(2)]
     n_rings = len(rings)
     operands = (
         resid,
@@ -618,8 +676,10 @@
             vmem((slots, width), BF16),
             dma((len(operands),)),
             dma((2,)),
+            pltpu.SemaphoreType.REGULAR,
+            pltpu.SemaphoreType.REGULAR,
             dma((2,)),
-            dma((chunks,)),
+            dma((n_sp,)),
             dma((1,)),
             dma((1,)),
             dma((n_rings,)),
@@ -628,8 +688,8 @@
             dma((n_rings, hops)),
             dma((1,)),
             dma((chunks,)),
-            dma((chunks, hops)),
-            dma((chunks, hops)),
+            dma((chunks * 2, hops)),
+            dma((chunks * 2, hops)),
         ],
         compiler_params=pltpu.CompilerParams(
             collective_id=0,

time: 128 us -> 134 us (1.047)
  the two profiles are of different devices: /device:TPU:80 before, /device:TPU:65 now
where the time goes in v3:
time: 134 us
  Pallas kernels  132 us (99%)
  other arithmetic  1.54 us (1%)
    pallas_call x1, Pallas kernels, per_device(): pl.pallas_call(functools.partial(layer_kernel, n_sp, n_tp, cap, rings), o...  132 us

profile of v3, /device:TPU:65, one launch (start us, length us, event | category | flops | bytes accessed | tf_op | source)
XLA Modules:
  0.0 133.7 jit_solution(8565220308693434258)
XLA Ops:
  0.0 132.1 %layer.1 = f32[16,2048]{1,0:T(8,128)} custom-call(bf16[16,2048]{1,0:T(8,128)(2,1)} %resid_h.1, bf16[256,128]{1,0:T(8,128)(2,1)} %gate_b_h.1, bf16[256,128]{1,0:T(8,128)(2,1)} %gate_c_h.1, bf16[256,128]{1,0:T(8,128)(2,1)} %value_h.1, bf16[3,128]{1,0:T(4,128)(2,1)} %taps_h.1, s32[2,128]{1,0:T(2,128)} %bitcast.5, bf16[128,2048]{1,0:T(8,128)(2,1)} %out_w_h.1, ...), custom_call_target="tpu_custom_call" | custom-call | tf_op jit(solution)/shard_map/layer/pallas_call | solution.py:646
  132.1 1.5 %convert_element_type.3 = bf16[16,2048]{1,0:T(8,128)(2,1)} convert(f32[16,2048]{1,0:T(8,128)} %layer.1) | non-fusion elementwise | flops 32768 | bytes 196608 | tf_op jit(solution)/shard_map/convert_element_type | solution.py:701

commit v4 on v3

--- a/solution.py
+++ b/solution.py
@@ -97,19 +97,17 @@
     load_sem,
     halo_sem,
     below_sem,
-    above_sem,
+    all_sem,
     z_send,
     z_recv,
     back_recv,
     pair_send,
     pair_recv,
     ring_send,
-    rr_recv,
-    rl_recv,
+    r_recv,
     gather_send,
     d_recv,
-    ar_recv,
-    al_recv,
+    a_recv,
 ):
     tok, ch = gate_b.shape
     rows, width = resid.shape
@@ -153,18 +151,11 @@
         pltpu.make_async_copy(ref, ref, sem).wait()
 
     barrier = pltpu.get_barrier_semaphore()
-    greeted = [partner, right, left]
+    greeted = [partner, right, left, along(-1), along(1)]
     for dev in greeted:
         pl.semaphore_signal(barrier, inc=1, device_id=dev, device_id_type=MESH)
-    has_below, has_above = sp > 0, sp < n_sp - 1
-
-    @pl.when(has_below)
-    def _():
-        pl.semaphore_signal(barrier, inc=1, device_id=along(-1), device_id_type=MESH)
-
-    @pl.when(has_above)
-    def _():
-        pl.semaphore_signal(barrier, inc=1, device_id=along(1), device_id_type=MESH)
+    last = n_sp - 1
+    has_below, has_above = sp > 0, sp < last
 
     loads = {}
     for i, (name, src, dst) in enumerate(
@@ -202,15 +193,30 @@
     halo_s[pl.ds(8, 8), :] = ext_ids[pl.ds(tok, 8), :]
 
     with jax.named_scope("barrier"):
-        pl.semaphore_wait(
-            barrier,
-            len(greeted) + jnp.where(has_below, 1, 0) + jnp.where(has_above, 1, 0),
-        )
+        pl.semaphore_wait(barrier, len(greeted))
     halo = remote(halo_s, halo_r, halo_sem.at[0], halo_sem.at[1], along(1))
 
     @pl.when(has_above)
     def _():
         halo.start()
+
+    with jax.named_scope("chain"):
+
+        @pl.when(sp > 2)
+        def _():
+            pl.semaphore_wait(below_sem, 1)
+
+        @pl.when((sp >= 2) & has_above)
+        def _():
+            pl.semaphore_signal(
+                below_sem, inc=1, device_id=along(1), device_id_type=MESH
+            )
+
+        @pl.when(sp == 0)
+        def _():
+            pl.semaphore_signal(
+                all_sem, inc=1, device_id=along(-1), device_id_type=MESH
+            )
 
     ext[pl.ds(0, 8), :] = jnp.zeros((8, ch), F32)
     ext_ids[pl.ds(0, 8), :] = jnp.full((8, LANES), -1.0, F32)
@@ -222,24 +228,6 @@
         halo.wait_recv()
         ext[pl.ds(0, 8), :] = halo_r[pl.ds(0, 8), :]
         ext_ids[pl.ds(0, 8), :] = halo_r[pl.ds(8, 8), :]
-
-    @pl.when(has_below)
-    def _():
-        pl.semaphore_wait(below_sem, 1)
-
-    @pl.when(has_above)
-    def _():
-        pl.semaphore_signal(
-            below_sem, inc=1, device_id=along(1), device_id_type=MESH
-        )
-
-    for d in range(1, n_sp):
-
-        @pl.when(sp >= d)
-        def _():
-            pl.semaphore_signal(
-                above_sem, inc=1, device_id=along(-d), device_id_type=MESH
-            )
 
     here = ext_ids[pl.ds(8, tok), :]
     tap_rows = taps[...].astype(F32)
@@ -272,6 +260,13 @@
             partner,
         )
 
+    def hop_wait(k, h):
+        _, at, cols = rings[k]
+        settle(
+            pair_r.at[0, pl.ds(0, TILE if h == 1 else 2 * TILE), pl.ds(at, cols)],
+            r_recv.at[k, h - 1],
+        )
+
     def ring_step(k, h):
         with jax.named_scope(f"rs{k}_{h}"):
             ring_hop(k, h)
@@ -288,15 +283,12 @@
         if h == 1:
             ring[k, "pair"].wait_recv()
             ring_s[s, hops, :, all_c] = share(hops, all_c).astype(BF16)
-        for name, buf, sem, dev, early, late in (
-            ("r", ring_r, rr_recv, right, lo, hi),
-            ("l", ring_l, rl_recv, left, hi, lo),
+        else:
+            hop_wait(k, h - 1)
+        for buf, dev, early, late, o in (
+            (ring_r, right, lo, hi, hops + 1 - h),
+            (ring_l, left, hi, lo, (chips - hops - 1 + h) % chips),
         ):
-            o = hops + 1 - h
-            if name == "l":
-                o = (chips - o) % chips
-            if h > 1:
-                ring[k, name, h - 1].wait_recv()
             if h == 2:
                 ring_s[s, o, :, early] = (
                     share(o, early) + buf[s, 0, :, early].astype(F32)
@@ -307,11 +299,11 @@
                     share(o, all_c) + buf[s, h - 2, :, all_c].astype(F32)
                 ).astype(BF16)
             c = early if h == 1 else all_c
-            ring[k, name, h] = send(
+            send(
                 ring_s.at[s, o, :, c],
                 buf.at[s, h - 1, :, c],
                 ring_send.at[0],
-                sem.at[k, h - 1],
+                r_recv.at[k, h - 1],
                 dev,
             )
 
@@ -319,8 +311,7 @@
         with jax.named_scope(f"re{k}"):
             s, at, cols = rings[k]
             c = pl.ds(at, cols)
-            ring[k, "r", hops].wait_recv()
-            ring[k, "l", hops].wait_recv()
+            hop_wait(k, hops)
             return (
                 keep[s, pl.ds(0, TILE), c]
                 + pair_r[s, pl.ds(0, TILE), c].astype(F32)
@@ -342,6 +333,14 @@
                 sel[1], ow[:, c], preferred_element_type=F32
             ).astype(BF16)
         pair_start(k)
+    @pl.when(sp == last)
+    def _():
+        pl.semaphore_wait(all_sem, 1)
+        for there in range(last):
+            pl.semaphore_signal(
+                all_sem, inc=1, device_id={"sp": there}, device_id_type=MESH
+            )
+
     for n in range(width // step_w):
         c = pl.ds(n * step_w, step_w)
         keep[0, :, c] = jnp.dot(sel[0], ow[:, c], preferred_element_type=F32)
@@ -408,7 +407,7 @@
 
         @pl.when(has_above)
         def _():
-            pl.semaphore_wait(above_sem, n_sp - 1 - sp)
+            pl.semaphore_wait(all_sem, 1)
 
     for p in range(1, n_sp):
         d = (p + 1) // 2 if p % 2 else -(p // 2)
@@ -421,7 +420,6 @@
             {"sp": there},
         )
 
-    gather = {}
     came = set()
 
     def block(cc, other, o):
@@ -460,21 +458,19 @@
                     pl.ds(cc * span + b, TILE, stride=folds), :
                 ].astype(BF16)
         elif h > 1:
-            gather[cc, part, "r", h - 1].wait_recv()
-            gather[cc, part, "l", h - 1].wait_recv()
-        k = cc * 2 + part
-        for name, sign, dev, sem, half in (
-            ("r", -1, right, ar_recv, 0),
-            ("l", 1, left, al_recv, 1),
-        ):
+            settle(
+                xbuf.at[pl.ds(0, 2 * TILE), pl.ds(0, part_w)],
+                a_recv.at[cc * 2 + part, h - 2],
+            )
+        for sign, dev, half in ((-1, right, 0), (1, left, 1)):
             c = pl.ds(part * part_w, part_w)
             if h == hops:
                 c = pl.ds(part * part_w + half * (part_w // 2), part_w // 2)
-            gather[cc, part, name, h] = send(
+            send(
                 xbuf.at[block(cc, 0, sign * (h - 1)), c],
                 xbuf.at[block(cc, 0, sign * h), c],
                 gather_send.at[0],
-                sem.at[k, h - 1],
+                a_recv.at[cc * 2 + part, h - 1],
                 dev,
             )
         to_partner(cc, part, 1 - h)
@@ -483,8 +479,10 @@
 
     def gather_last(cc, part):
         with jax.named_scope(f"al{cc}{part}"):
-            gather[cc, part, "r", hops].wait_recv()
-            gather[cc, part, "l", hops].wait_recv()
+            settle(
+                xbuf.at[pl.ds(0, TILE), pl.ds(0, part_w)],
+                a_recv.at[cc * 2 + part, hops - 1],
+            )
             to_partner(cc, part, hops)
 
     def experts(cc):
@@ -685,10 +683,8 @@
             dma((n_rings,)),
             dma((1,)),
             dma((n_rings, hops)),
-            dma((n_rings, hops)),
             dma((1,)),
             dma((chunks,)),
-            dma((chunks * 2, hops)),
             dma((chunks * 2, hops)),
         ],
         compiler_params=pltpu.CompilerParams(

time: 134 us -> 132 us (0.985)
  the two profiles are of different devices: /device:TPU:65 before, /device:TPU:80 now
where the time goes in v4:
time: 132 us
  Pallas kernels  130 us (98%)
  other arithmetic  1.54 us (1%)
    pallas_call x1, Pallas kernels, per_device(): pl.pallas_call(functools.partial(layer_kernel, n_sp, n_tp, cap, rings), o...  130 us

profile of v4, /device:TPU:80, one launch (start us, length us, event | category | flops | bytes accessed | tf_op | source)
XLA Modules:
  0.0 132.0 jit_solution(16612992217870948689)
XLA Ops:
  0.0 130.4 %layer.1 = f32[16,2048]{1,0:T(8,128)} custom-call(bf16[16,2048]{1,0:T(8,128)(2,1)} %resid_h.1, bf16[256,128]{1,0:T(8,128)(2,1)} %gate_b_h.1, bf16[256,128]{1,0:T(8,128)(2,1)} %gate_c_h.1, bf16[256,128]{1,0:T(8,128)(2,1)} %value_h.1, bf16[3,128]{1,0:T(4,128)(2,1)} %taps_h.1, s32[2,128]{1,0:T(2,128)} %bitcast.5, bf16[128,2048]{1,0:T(8,128)(2,1)} %out_w_h.1, ...), custom_call_target="tpu_custom_call" | custom-call | tf_op jit(solution)/shard_map/layer/pallas_call | solution.py:644
  130.4 1.5 %convert_element_type.3 = bf16[16,2048]{1,0:T(8,128)(2,1)} convert(f32[16,2048]{1,0:T(8,128)} %layer.1) | non-fusion elementwise | flops 32768 | bytes 196608 | tf_op jit(solution)/shard_map/convert_element_type | solution.py:697

commit v5 on v4

--- a/solution.py
+++ b/solution.py
@@ -17,17 +17,17 @@
 ORDER = (
     (0, 0, 0, 1), (0, 0, 1, 1), (0, 1, 0, 1), (0, 1, 1, 1), (0, 0, 0, 2),
     (0, 0, 1, 2), (0, 1, 0, 2), (0, 1, 1, 2), (0, 0, 0, 3), (0, 0, 1, 3),
-    (0, 1, 0, 3), (0, 2, 0, 1), (0, 2, 1, 1), (0, 0, 0, 4), (0, 1, 1, 3),
-    (0, 0, 1, 4), (0, 1, 0, 4), (0, 2, 0, 2), (0, 2, 1, 2), (4, 0, 0),
-    (4, 0, 1), (4, 1, 0), (0, 2, 0, 3), (0, 2, 1, 3), (0, 1, 1, 4),
-    (1, 0), (0, 2, 0, 4), (0, 2, 1, 4), (4, 1, 1), (2, 0, 0, 1),
-    (2, 0, 1, 1), (4, 2, 0), (4, 2, 1), (2, 0, 0, 2), (2, 0, 1, 2),
-    (1, 2), (1, 1), (2, 2, 0, 1), (2, 2, 1, 1), (2, 1, 0, 1),
-    (2, 1, 1, 1), (2, 0, 0, 3), (2, 0, 1, 3), (2, 2, 0, 2), (2, 2, 1, 2),
-    (2, 1, 0, 2), (2, 1, 1, 2), (2, 0, 0, 4), (2, 2, 0, 3), (2, 2, 1, 3),
-    (2, 1, 0, 3), (2, 1, 1, 3), (3, 0, 0), (2, 2, 0, 4), (2, 2, 1, 4),
-    (2, 1, 0, 4), (2, 1, 1, 4), (2, 0, 1, 4), (3, 2, 0), (3, 2, 1),
-    (3, 1, 0), (3, 1, 1), (3, 0, 1),
+    (0, 1, 0, 3), (0, 2, 0, 1), (0, 2, 1, 1), (0, 1, 1, 3), (0, 0, 0, 4),
+    (0, 0, 1, 4), (0, 1, 0, 4), (0, 2, 0, 2), (0, 2, 1, 2), (0, 1, 1, 4),
+    (4, 0, 0), (4, 0, 1), (4, 1, 0), (0, 2, 0, 3), (0, 2, 1, 3),
+    (4, 1, 1), (1, 0), (1, 1), (0, 2, 0, 4), (0, 2, 1, 4),
+    (2, 0, 0, 1), (2, 0, 1, 1), (2, 1, 0, 1), (2, 1, 1, 1), (4, 2, 0),
+    (4, 2, 1), (1, 2), (2, 1, 0, 2), (2, 2, 0, 1), (2, 2, 1, 1),
+    (2, 1, 1, 2), (2, 0, 0, 2), (2, 0, 1, 2), (2, 2, 0, 2), (2, 2, 1, 2),
+    (2, 1, 0, 3), (2, 1, 1, 3), (2, 0, 0, 3), (2, 2, 0, 3), (2, 2, 1, 3),
+    (2, 0, 1, 3), (2, 1, 0, 4), (2, 1, 1, 4), (2, 2, 0, 4), (2, 2, 1, 4),
+    (2, 0, 0, 4), (2, 0, 1, 4), (3, 1, 0), (3, 1, 1), (3, 2, 0),
+    (3, 2, 1), (3, 0, 0), (3, 0, 1),
 )
 BF16 = jnp.bfloat16
 F32 = jnp.float32
@@ -400,8 +400,11 @@
         ]
     folded = fold[...].astype(BF16)
     zs[...] = folded
-    my_piece = pl.ds(pl.multiple_of(sp * piece, piece), piece)
-    zr[my_piece, :] = zs[my_piece, :]
+    shift = 3 * n_sp // 16
+    my_pos = lax.rem(sp + n_sp - shift, n_sp)
+    as_source = pl.ds(pl.multiple_of(my_pos * piece, piece), piece)
+    as_expert = pl.ds(pl.multiple_of(sp * piece, piece), piece)
+    zr[as_source, :] = zs[as_expert, :]
 
     with jax.named_scope("above"):
 
@@ -414,9 +417,9 @@
         there = lax.rem(sp + d + n_sp, n_sp)
         send(
             zs.at[pl.ds(pl.multiple_of(there * piece, piece), piece), :],
-            zr.at[my_piece, :],
+            zr.at[as_source, :],
             z_send.at[0],
-            z_recv.at[sp],
+            z_recv.at[my_pos],
             {"sp": there},
         )
 
@@ -442,7 +445,7 @@
             gather_step(cc, part, h)
 
     def arrive(src):
-        @pl.when(sp != src)
+        @pl.when(my_pos != src)
         def _():
             settle(zr.at[pl.ds(src * piece, piece), :], z_recv.at[src])
 
@@ -534,14 +537,16 @@
             if p not in back_sent and needs <= finished:
                 back_sent.add(p)
 
-                @pl.when(sp != p)
+                owner = (p + shift) % n_sp
+
+                @pl.when(sp != owner)
                 def _():
                     send(
                         bs.at[pl.ds(p * piece, piece), :],
-                        br.at[my_piece, :],
+                        br.at[as_expert, :],
                         z_send.at[1],
                         back_recv.at[0],
-                        {"sp": p},
+                        {"sp": owner},
                     )
 
     for name in ("wg", "wu", "wd"):
@@ -557,7 +562,7 @@
             ring_step(set_rings[op[1] + 1][op[2]], op[3])
         else:
             finish(*op[1:])
-    br[my_piece, :] = bs[my_piece, :]
+    br[as_expert, :] = bs[as_source, :]
 
     far = (n_sp - 1) * piece
     ring_rows = (2 * hops - 1) * TILE

time: 132 us -> 121 us (0.917)
  Pallas kernels: 130 us -> 119 us
    pallas_call x1, Pallas kernels: 130 us -> 119 us  [per_device(): pl.pallas_call(functools.partial(layer_kernel, n_sp, n_tp, cap, rings), o...]
where the time goes in v5:
time: 121 us; the launch traced here: 120 us
  Pallas kernels  119 us (98%)
  other arithmetic  1.54 us (1%)
    pallas_call x1, Pallas kernels, per_device(): pl.pallas_call(functools.partial(layer_kernel, n_sp, n_tp, cap, rings), o...  119 us

profile of v5, /device:TPU:80, one launch (start us, length us, event | category | flops | bytes accessed | tf_op | source)
XLA Modules:
  0.0 120.5 jit_solution(15455585059168958671)
XLA Ops:
  0.0 118.9 %layer.1 = f32[16,2048]{1,0:T(8,128)} custom-call(bf16[16,2048]{1,0:T(8,128)(2,1)} %resid_h.1, bf16[256,128]{1,0:T(8,128)(2,1)} %gate_b_h.1, bf16[256,128]{1,0:T(8,128)(2,1)} %gate_c_h.1, bf16[256,128]{1,0:T(8,128)(2,1)} %value_h.1, bf16[3,128]{1,0:T(4,128)(2,1)} %taps_h.1, s32[2,128]{1,0:T(2,128)} %bitcast.5, bf16[128,2048]{1,0:T(8,128)(2,1)} %out_w_h.1, ...), custom_call_target="tpu_custom_call" | custom-call | tf_op jit(solution)/shard_map/layer/pallas_call | solution.py:649
  118.9 1.5 %convert_element_type.3 = bf16[16,2048]{1,0:T(8,128)(2,1)} convert(f32[16,2048]{1,0:T(8,128)} %layer.1) | non-fusion elementwise | flops 32768 | bytes 196608 | tf_op jit(solution)/shard_map/convert_element_type | solution.py:702

commit v6 on v5

--- a/solution.py
+++ b/solution.py
@@ -16,18 +16,18 @@
 
 ORDER = (
     (0, 0, 0, 1), (0, 0, 1, 1), (0, 1, 0, 1), (0, 1, 1, 1), (0, 0, 0, 2),
-    (0, 0, 1, 2), (0, 1, 0, 2), (0, 1, 1, 2), (0, 0, 0, 3), (0, 0, 1, 3),
-    (0, 1, 0, 3), (0, 2, 0, 1), (0, 2, 1, 1), (0, 1, 1, 3), (0, 0, 0, 4),
-    (0, 0, 1, 4), (0, 1, 0, 4), (0, 2, 0, 2), (0, 2, 1, 2), (0, 1, 1, 4),
-    (4, 0, 0), (4, 0, 1), (4, 1, 0), (0, 2, 0, 3), (0, 2, 1, 3),
-    (4, 1, 1), (1, 0), (1, 1), (0, 2, 0, 4), (0, 2, 1, 4),
-    (2, 0, 0, 1), (2, 0, 1, 1), (2, 1, 0, 1), (2, 1, 1, 1), (4, 2, 0),
-    (4, 2, 1), (1, 2), (2, 1, 0, 2), (2, 2, 0, 1), (2, 2, 1, 1),
-    (2, 1, 1, 2), (2, 0, 0, 2), (2, 0, 1, 2), (2, 2, 0, 2), (2, 2, 1, 2),
-    (2, 1, 0, 3), (2, 1, 1, 3), (2, 0, 0, 3), (2, 2, 0, 3), (2, 2, 1, 3),
-    (2, 0, 1, 3), (2, 1, 0, 4), (2, 1, 1, 4), (2, 2, 0, 4), (2, 2, 1, 4),
-    (2, 0, 0, 4), (2, 0, 1, 4), (3, 1, 0), (3, 1, 1), (3, 2, 0),
-    (3, 2, 1), (3, 0, 0), (3, 0, 1),
+    (0, 0, 1, 2), (0, 1, 0, 2), (0, 1, 1, 2), (0, 2, 0, 1), (0, 2, 1, 1),
+    (0, 0, 0, 3), (0, 0, 1, 3), (0, 1, 0, 3), (0, 1, 1, 3), (0, 2, 0, 2),
+    (0, 2, 1, 2), (0, 0, 0, 4), (0, 0, 1, 4), (0, 1, 0, 4), (0, 1, 1, 4),
+    (0, 2, 0, 3), (0, 2, 1, 3), (4, 0, 0), (4, 0, 1), (4, 1, 0),
+    (1, 0), (4, 1, 1), (0, 2, 0, 4), (0, 2, 1, 4), (1, 1),
+    (2, 0, 0, 1), (2, 0, 1, 1), (4, 2, 0), (4, 2, 1), (2, 1, 0, 1),
+    (2, 1, 1, 1), (1, 2), (2, 0, 0, 2), (2, 0, 1, 2), (2, 2, 0, 1),
+    (2, 2, 1, 1), (2, 1, 0, 2), (2, 1, 1, 2), (2, 0, 0, 3), (2, 2, 0, 2),
+    (2, 2, 1, 2), (2, 0, 1, 3), (2, 1, 0, 3), (2, 1, 1, 3), (2, 0, 0, 4),
+    (2, 2, 0, 3), (2, 2, 1, 3), (2, 0, 1, 4), (2, 1, 0, 4), (2, 1, 1, 4),
+    (3, 0, 0), (2, 2, 0, 4), (2, 2, 1, 4), (3, 0, 1), (3, 1, 0),
+    (3, 1, 1), (3, 2, 0), (3, 2, 1),
 )
 BF16 = jnp.bfloat16
 F32 = jnp.float32
@@ -412,7 +412,7 @@
         def _():
             pl.semaphore_wait(all_sem, 1)
 
-    for p in range(1, n_sp):
+    for p in reversed(range(1, n_sp)):
         d = (p + 1) // 2 if p % 2 else -(p // 2)
         there = lax.rem(sp + d + n_sp, n_sp)
         send(
@@ -499,14 +499,15 @@
             g = jnp.dot(x, wg[...], preferred_element_type=F32)
             u = jnp.dot(x, wu[...], preferred_element_type=F32)
             hid[...] = (g / (1.0 + jnp.exp(-g)) * u).astype(BF16)
-            for n in range(width // step_w):
-                c = pl.ds(n * step_w, step_w)
-                pair_s[s, :, c] = jnp.dot(
-                    hid[pl.ds(own_rows, own_rows), :],
-                    wd[:, c],
-                    preferred_element_type=F32,
-                ).astype(BF16)
             for k in set_rings[s]:
+                _, at, cols = rings[k]
+                for n in range(cols // step_w):
+                    c = pl.ds(at + n * step_w, step_w)
+                    pair_s[s, :, c] = jnp.dot(
+                        hid[pl.ds(own_rows, own_rows), :],
+                        wd[:, c],
+                        preferred_element_type=F32,
+                    ).astype(BF16)
                 pair_start(k)
             for n in range(width // step_w):
                 c = pl.ds(n * step_w, step_w)

time: 121 us -> 121 us (level)
  no operation moved by 1% of the time
where the time goes in v6:
time: 121 us; the launch traced here: 120 us
  Pallas kernels  119 us (98%)
  other arithmetic  1.54 us (1%)
    pallas_call x1, Pallas kernels, per_device(): pl.pallas_call(functools.partial(layer_kernel, n_sp, n_tp, cap, rings), o...  119 us

profile of v6, /device:TPU:80, one launch (start us, length us, event | category | flops | bytes accessed | tf_op | source)
XLA Modules:
  0.0 120.4 jit_solution(11552129266124451207)
XLA Ops:
  0.0 118.9 %layer.1 = f32[16,2048]{1,0:T(8,128)} custom-call(bf16[16,2048]{1,0:T(8,128)(2,1)} %resid_h.1, bf16[256,128]{1,0:T(8,128)(2,1)} %gate_b_h.1, bf16[256,128]{1,0:T(8,128)(2,1)} %gate_c_h.1, bf16[256,128]{1,0:T(8,128)(2,1)} %value_h.1, bf16[3,128]{1,0:T(4,128)(2,1)} %taps_h.1, s32[2,128]{1,0:T(2,128)} %bitcast.5, bf16[128,2048]{1,0:T(8,128)(2,1)} %out_w_h.1, ...), custom_call_target="tpu_custom_call" | custom-call | tf_op jit(solution)/shard_map/layer/pallas_call | solution.py:650
  118.9 1.5 %convert_element_type.3 = bf16[16,2048]{1,0:T(8,128)(2,1)} convert(f32[16,2048]{1,0:T(8,128)} %layer.1) | non-fusion elementwise | flops 32768 | bytes 196608 | tf_op jit(solution)/shard_map/convert_element_type | solution.py:703

commit v7 on v6

--- a/solution.py
+++ b/solution.py
@@ -20,13 +20,13 @@
     (0, 0, 0, 3), (0, 0, 1, 3), (0, 1, 0, 3), (0, 1, 1, 3), (0, 2, 0, 2),
     (0, 2, 1, 2), (0, 0, 0, 4), (0, 0, 1, 4), (0, 1, 0, 4), (0, 1, 1, 4),
     (0, 2, 0, 3), (0, 2, 1, 3), (4, 0, 0), (4, 0, 1), (4, 1, 0),
-    (1, 0), (4, 1, 1), (0, 2, 0, 4), (0, 2, 1, 4), (1, 1),
-    (2, 0, 0, 1), (2, 0, 1, 1), (4, 2, 0), (4, 2, 1), (2, 1, 0, 1),
+    (1, 0), (4, 1, 1), (0, 2, 0, 4), (0, 2, 1, 4), (2, 0, 0, 1),
+    (2, 0, 1, 1), (1, 1), (4, 2, 0), (4, 2, 1), (2, 1, 0, 1),
     (2, 1, 1, 1), (1, 2), (2, 0, 0, 2), (2, 0, 1, 2), (2, 2, 0, 1),
-    (2, 2, 1, 1), (2, 1, 0, 2), (2, 1, 1, 2), (2, 0, 0, 3), (2, 2, 0, 2),
-    (2, 2, 1, 2), (2, 0, 1, 3), (2, 1, 0, 3), (2, 1, 1, 3), (2, 0, 0, 4),
-    (2, 2, 0, 3), (2, 2, 1, 3), (2, 0, 1, 4), (2, 1, 0, 4), (2, 1, 1, 4),
-    (3, 0, 0), (2, 2, 0, 4), (2, 2, 1, 4), (3, 0, 1), (3, 1, 0),
+    (2, 2, 1, 1), (2, 1, 0, 2), (2, 1, 1, 2), (2, 0, 0, 3), (2, 0, 1, 3),
+    (2, 2, 0, 2), (2, 2, 1, 2), (2, 1, 0, 3), (2, 1, 1, 3), (2, 0, 0, 4),
+    (2, 0, 1, 4), (2, 2, 0, 3), (2, 2, 1, 3), (2, 1, 0, 4), (2, 1, 1, 4),
+    (3, 0, 0), (3, 0, 1), (2, 2, 0, 4), (2, 2, 1, 4), (3, 1, 0),
     (3, 1, 1), (3, 2, 0), (3, 2, 1),
 )
 BF16 = jnp.bfloat16

time: 121 us -> 121 us (level)
  no operation moved by 1% of the time
where the time goes in v7:
time: 121 us
  Pallas kernels  120 us (99%)
  other arithmetic  1.54 us (1%)
    pallas_call x1, Pallas kernels, per_device(): pl.pallas_call(functools.partial(layer_kernel, n_sp, n_tp, cap, rings), o...  120 us

profile of v7, /device:TPU:80, one launch (start us, length us, event | category | flops | bytes accessed | tf_op | source)
XLA Modules:
  0.0 121.2 jit_solution(1402671827997512601)
XLA Ops:
  0.0 119.7 %layer.1 = f32[16,2048]{1,0:T(8,128)} custom-call(bf16[16,2048]{1,0:T(8,128)(2,1)} %resid_h.1, bf16[256,128]{1,0:T(8,128)(2,1)} %gate_b_h.1, bf16[256,128]{1,0:T(8,128)(2,1)} %gate_c_h.1, bf16[256,128]{1,0:T(8,128)(2,1)} %value_h.1, bf16[3,128]{1,0:T(4,128)(2,1)} %taps_h.1, s32[2,128]{1,0:T(2,128)} %bitcast.5, bf16[128,2048]{1,0:T(8,128)(2,1)} %out_w_h.1, ...), custom_call_target="tpu_custom_call" | custom-call | tf_op jit(solution)/shard_map/layer/pallas_call | solution.py:650
  119.7 1.5 %convert_element_type.3 = bf16[16,2048]{1,0:T(8,128)(2,1)} convert(f32[16,2048]{1,0:T(8,128)} %layer.1) | non-fusion elementwise | flops 32768 | bytes 196608 | tf_op jit(solution)/shard_map/convert_element_type | solution.py:703
